TPU v7x, 256 devices: a whole 4x4x8 slice. The times are simulated.
256 devices in a mesh: ep: 64 (over z, x, core), tp: 4 (over y).
Axes of the slice: x: 4, y: 4, z: 8, core: 2. Of those that a mesh axis runs over, the one named last changes fastest.
Arguments:
- conv_input: bfloat16 [32768, 2048], P(('ep', 'tp')), may hold values from -6 to 6
- conv_kernel: float32 [31, 2048], replicated, may hold values from -1 to 1
- conv_gain: float32 [2048], replicated, may hold values from 0.1 to 1.9
- out_weight: bfloat16 [2048, 2048], P(None, 'tp'), may hold values from -0.125 to 0.125
- moe_input: bfloat16 [32768, 2048], P(('ep', 'tp')), may hold values from -6 to 6
- moe_gain: float32 [2048], replicated, may hold values from 0.1 to 1.9
- expert_gate: bfloat16 [64, 2048, 2048], P('ep', None, 'tp'), may hold values from -0.125 to 0.125
- expert_up: bfloat16 [64, 2048, 2048], P('ep', None, 'tp'), may hold values from -0.125 to 0.125
- expert_down: bfloat16 [64, 2048, 2048], P('ep', 'tp'), may hold values from -0.125 to 0.125
- shared_gate: bfloat16 [2048, 128], replicated, may hold values from -0.125 to 0.125
- shared_up: bfloat16 [2048, 128], replicated, may hold values from -0.125 to 0.125
- shared_down: bfloat16 [128, 2048], replicated, may hold values from -0.5 to 0.5
- expert_index: int32 [32768, 2], P('ep'), may hold values from 0 to 63, all different within a row; in each aligned block of 128 rows (0 to 127, 128 to 255, ...) at most 6 rows name the same one
- routing_weight: float32 [32768, 2], P(('ep', 'tp')), may hold values from 0.25 to 1.5
Outputs:
- conv_out: bfloat16 [32768, 2048], P('ep', 'tp')
- moe_out: bfloat16 [32768, 2048], P(('ep', 'tp'))
Inputs may be any that keep to these rules, and one draw needn't show every extreme that they name: `expert_index`: each row names 2 different experts. In each aligned block of 128 rows no expert is named by more than 6 of the rows, and in some blocks one expert is named by exactly 6 rows.
All inputs are finite; a program needn't handle non-finite values.
Results may differ from a plain program's by a relative error of at most 0.009.
Values may be sent and summed in bfloat16 or wider, within the bound.
A program may use at most 128 MiB of HBM per device.

v0:
```python
import jax
import jax.numpy as jnp
from jax import lax
from jax.sharding import PartitionSpec as P

NORM_EPS = 1e-05


def passed_along(block, axis, distance):
    devices = range(lax.axis_size(axis))
    route = [(i - distance, i) for i in devices if i - distance in devices]
    return lax.ppermute(block, axis, route)


def laid_out(pieces, dim):
    lengths = list(pieces.shape[1:])
    lengths[dim] *= pieces.shape[0]
    return jnp.moveaxis(pieces, 0, dim).reshape(lengths)


def on_gathered_pieces(shard, axis, dim, apply, out_dim):
    size, rows = (lax.axis_size(axis), shard.shape[dim])
    count = 2 if rows % 2 == 0 else 1
    finished, length = ([], rows // count)
    for k in range(count):
        slab = lax.slice_in_dim(shard, k * length, (k + 1) * length, axis=dim)
        starts = jnp.arange(size) * rows + k * length
        finished.append(jax.vmap(apply)(lax.all_gather(slab, axis), starts))
    return laid_out(jnp.concatenate(finished, axis=out_dim + 1), out_dim)


def layer_scale(row_data, gain_vec):
    values = row_data.astype(jnp.float32)
    center = values - jnp.mean(values, axis=-1, keepdims=True)
    spread = jnp.mean(center * center, axis=-1, keepdims=True)
    return center * lax.rsqrt(spread + NORM_EPS) * gain_vec


def depthwise(padded, kernel, length):
    running = jnp.zeros((length, padded.shape[1]), jnp.float32)
    for offset in range(kernel.shape[0]):
        running = running + padded[offset : offset + length].astype(jnp.float32) * kernel[offset]
    return running


def slot_table(block_index, experts, slot_count):
    onehot = (
        block_index[:, :, None] == jnp.arange(experts, dtype=jnp.int32)[None, None, :]
    ).astype(jnp.int32)
    before = jnp.cumsum(onehot, axis=1) - onehot
    position = jnp.sum(before * onehot, axis=2)
    return block_index * slot_count + position


def fill_slots(row_data, entry_slot, top_count, total_slots):
    block_count = entry_slot.shape[0]
    entries = entry_slot.shape[1]
    block_ids = jnp.arange(block_count, dtype=jnp.int32)[:, None]
    source = jnp.arange(entries, dtype=jnp.int32)[None, :] // top_count
    slot_row = (
        jnp.zeros((block_count, total_slots), jnp.int32).at[block_ids, entry_slot].set(source)
    )
    filled = jnp.zeros((block_count, total_slots), jnp.int32).at[block_ids, entry_slot].set(1)
    picked = row_data[block_ids, slot_row]
    return jnp.where(filled[:, :, None] > 0, picked, jnp.zeros((), row_data.dtype))


def gated(row_data, gate_weight, up_weight):
    gate_proj = jnp.dot(row_data, gate_weight, preferred_element_type=jnp.float32)
    up_proj = jnp.dot(row_data, up_weight, preferred_element_type=jnp.float32)
    return (jax.nn.silu(gate_proj) * up_proj).astype(jnp.bfloat16)


def on_device(
    conv_input,
    conv_kernel,
    conv_gain,
    out_weight,
    moe_input,
    moe_gain,
    expert_gate,
    expert_up,
    expert_down,
    shared_gate,
    shared_up,
    shared_down,
    expert_index,
    routing_weight,
):
    reach = conv_kernel.shape[0] - 1
    length = conv_input.shape[0]
    halo_rows = passed_along(conv_input[length - reach :], ("ep", "tp"), 1)
    padded = jnp.concatenate([halo_rows, conv_input], axis=0)
    mixed_rows = depthwise(padded, conv_kernel, length)
    normed = jax.nn.silu(layer_scale(mixed_rows, conv_gain)).astype(jnp.bfloat16)

    def project(row_piece, row_start):
        return jnp.dot(row_piece, out_weight, preferred_element_type=jnp.float32).astype(
            jnp.bfloat16
        )

    conv_out = on_gathered_pieces(normed, "tp", 0, project, 0)
    tp_parts = lax.axis_size("tp")
    tp_index = lax.axis_index("tp")
    ep_ranks = lax.axis_size("ep")
    tok_count = moe_input.shape[0]
    top_count = routing_weight.shape[1]
    model_width = moe_input.shape[1]
    experts = ep_ranks * expert_gate.shape[0]
    slot_count = 3 * tok_count * top_count // (2 * experts)
    total_slots = experts * slot_count
    normal = layer_scale(moe_input, moe_gain).astype(jnp.bfloat16)
    group_slots = slot_table(
        expert_index.reshape(tp_parts, tok_count * top_count), experts, slot_count
    )
    own_slots = lax.dynamic_index_in_dim(group_slots, tp_index, 0, keepdims=True)
    gate_local = expert_gate[0]
    up_local = expert_up[0]
    down_local = expert_down[0]
    own_rows = fill_slots(normal[None], own_slots, top_count, total_slots)
    own_rows = own_rows.reshape(ep_ranks, slot_count, model_width)
    arrived = lax.all_to_all(own_rows, "ep", split_axis=0, concat_axis=0, tiled=True)
    hidden = gated(
        lax.all_gather(
            arrived.reshape(ep_ranks * slot_count, model_width), "tp", axis=0, tiled=True
        ),
        gate_local,
        up_local,
    )
    row_piece = hidden
    summed = lax.psum_scatter(
        jnp.dot(row_piece, down_local, preferred_element_type=jnp.float32).astype(jnp.bfloat16),
        "tp",
        scatter_dimension=0,
        tiled=True,
    )
    returned = lax.all_to_all(
        summed.reshape(ep_ranks, slot_count, model_width),
        "ep",
        split_axis=0,
        concat_axis=0,
        tiled=True,
    )
    picked = returned.reshape(total_slots, model_width)[own_slots[0]]
    picked = picked.reshape(tok_count, top_count, model_width).astype(jnp.float32)
    routed = jnp.sum(picked * routing_weight[:, :, None], axis=1)
    shared_hidden = gated(normal, shared_gate, shared_up)
    shared_part = jnp.dot(shared_hidden, shared_down, preferred_element_type=jnp.float32)
    moe_out = (shared_part + routed).astype(jnp.bfloat16)
    return (conv_out, moe_out)


def solution(mesh):
    in_specs = (
        P(("ep", "tp"), None),
        P(),
        P(),
        P(None, "tp"),
        P(("ep", "tp"), None),
        P(),
        P("ep", None, "tp"),
        P("ep", None, "tp"),
        P("ep", "tp", None),
        P(),
        P(),
        P(),
        P("ep", None),
        P(("ep", "tp"), None),
    )
    out_specs = (P("ep", "tp"), P(("ep", "tp"), None))
    return jax.shard_map(
        on_device, mesh=mesh, in_specs=in_specs, out_specs=out_specs, check_vma=False
    )
```

profile of v0, /device:TPU:1, one launch (start us, length us, event | category | flops | bytes accessed | tf_op | source)
XLA Modules:
  0.0 341.9 jit_solution(2187914190546542407)
XLA Ops:
  8.6 2.4 reduce-window.6
  13.8 9.4 %gather_fusion = bf16[384,2048]{1,0:T(8,128)(2,1)} fusion(bf16[1,128,2048]{2,1,0:T(8,128)(2,1)S(1)} %fusion.77, s32[384]{0:T(512)S(1)} %fusion.69), kind=kCustom, calls=%fused_computation | custom fusion | bytes 3148800 | tf_op jit(solution)/shard_map/gather | solution.py:64
  23.2 3.7 %gather.9 = bf16[64,6,2048]{2,1,0:T(8,128)(2,1)} reshape(bf16[384,2048]{1,0:T(8,128)(2,1)} %gather_fusion) | data formatting | bytes 3145728 | tf_op jit(solution)/shard_map/gather | solution.py:64
  30.4 62.6 %all_to_all.10 = bf16[64,6,2048]{2,1,0:T(8,128)(2,1)} all-to-all(bf16[64,6,2048]{2,1,0:T(8,128)(2,1)S(1)} %broadcast_select_fusion), channel_id=1, replica_groups=mesh['ep'=64,'tp'=4] {'ep'}, dimensions={0} | all-to-all | bytes 3145728 | tf_op jit(solution)/shard_map/all_to_all | solution.py:122
  92.9 3.7 %reshape.171 = bf16[384,2048]{1,0:T(8,128)(2,1)} reshape(bf16[64,6,2048]{2,1,0:T(8,128)(2,1)} %all_to_all.10) | data formatting | bytes 3145728 | tf_op jit(solution)/shard_map/reshape | solution.py:125
  96.9 65.7 %all-gather.6.cloned.1.call-done = bf16[1536,2048]{1,0:T(8,128)(2,1)} async-done(((bf16[384,2048]{1,0:T(8,128)(2,1)}), bf16[1536,2048]{1,0:T(8,128)(2,1)}) %all-gather.6.cloned.1.call-update) | async-done | bytes 6291472 | tf_op jit(solution)/shard_map/all_gather | solution.py:124
  162.7 8.5 %fusion.4 = f32[1536,512]{1,0:T(8,128)} fusion(bf16[1536,2048]{1,0:T(8,128)(2,1)} %all-gather.6.cloned.1.call-done, bf16[1,2048,512]{2,1,0:T(8,128)(2,1)} %param.20), kind=kOutput, calls=%fused_computation.40 | convolution fusion | flops 3221225472 | bytes 11534336 | tf_op jit(solution)/shard_map/dot_general | solution.py:69
  171.2 11.8 %convolution_convert_fusion = bf16[1536,2048]{1,0:T(8,128)(2,1)} fusion(bf16[1,512,2048]{2,1,0:T(8,128)(2,1)S(1)} %copy-done, bf16[1536,2048]{1,0:T(8,128)(2,1)} %all-gather.6.cloned.1.call-done, f32[1536,512]{1,0:T(8,128)} %fusion.4, bf16[1,2048,512]{2,1,0:T(8,128)(2,1)} %param.21), kind=kOutput, calls=%fused_computation.4 | convolution fusion | flops 6450315264 | bytes 19922944 | tf_op jit(solution)/shard_map/dot_general | solution.py:132
  184.1 2.8 collective-permute-start
  187.0 4.5 %collective-permute-done = bf16[30,2048]{1,0:T(8,128)(2,1)S(1)} collective-permute-done((bf16[30,2048]{1,0:T(8,128)(2,1)S(1)}, bf16[30,2048]{1,0:T(8,128)(2,1)S(1)}, u32[]{:S(2)}, u32[]{:S(2)}) %collective-permute-start) | collective-permute-done | bytes 122912 | tf_op jit(solution)/shard_map/ppermute | solution.py:12
  191.6 4.8 %fusion.82 = (f32[128]{0:T(128)S(1)}, f32[128,2048]{1,0:T(8,128)S(1)}) fusion(f32[2048]{0:T(1024)S(1)} %bitcast.128, bf16[128,2048]{1,0:T(8,128)(2,1)S(1)} %copy-done.2, f32[2048]{0:T(1024)S(1)} %bitcast.129, bf16[30,2048]{1,0:T(8,128)(2,1)S(1)} %collective-permute-done, f32[2048]{0:T(1024)S(1)} %bitcast.100, f32[2048]{0:T(1024)S(1)} %bitcast.101, ...), kind=kLoop, calls=%fused_computation.170 | loop fusion | flops 47972224 | bytes 1950208 | tf_op jit(solution)/shard_map/reduce_sum | solution.py:34
  198.0 52.5 %reduce-scatter.2.cloned.1.call-done = bf16[384,2048]{1,0:T(8,128)(2,1)} async-done(((bf16[1536,2048]{1,0:T(8,128)(2,1)}), bf16[384,2048]{1,0:T(8,128)(2,1)}) %reduce-scatter.2.cloned.1.call-update) | async-done | bytes 1572880 | tf_op jit(solution)/shard_map/reduce_scatter | solution.py:131
  250.5 3.7 %reshape.172 = bf16[64,6,2048]{2,1,0:T(8,128)(2,1)} reshape(bf16[384,2048]{1,0:T(8,128)(2,1)} %reduce-scatter.2.cloned.1.call-done) | data formatting | bytes 3145728 | tf_op jit(solution)/shard_map/reshape | solution.py:138
  254.2 11.0 %all-to-all-start.1 = ((bf16[64,6,2048]{2,1,0:T(8,128)(2,1)}), bf16[64,6,2048]{2,1,0:T(8,128)(2,1)}, u32[]{:S(2)}, u32[]{:S(2)}) async-start(bf16[64,6,2048]{2,1,0:T(8,128)(2,1)} %reshape.172), calls=%async_computation.2 | async-start | bytes 4194304 | tf_op jit(solution)/shard_map/all_to_all | solution.py:137
  266.3 11.3 %all-gather.8.cloned.1.call-done = bf16[256,2048]{1,0:T(8,128)(2,1)} async-done(((bf16[64,2048]{1,0:T(8,128)(2,1)}), bf16[256,2048]{1,0:T(8,128)(2,1)}) %all-gather.8.cloned.1.call-update) | async-done | bytes 1048592 | tf_op jit(solution)/shard_map/all_gather | solution.py:28
  277.6 2.6 fusion.12
  280.2 26.4 %all-gather.10.cloned.1.call-done = bf16[256,2048]{1,0:T(8,128)(2,1)} async-done(((bf16[64,2048]{1,0:T(8,128)(2,1)}), bf16[256,2048]{1,0:T(8,128)(2,1)}) %all-gather.10.cloned.1.call-update) | async-done | bytes 1048592 | tf_op jit(solution)/shard_map/all_gather | solution.py:28
  306.6 2.6 fusion.15
  310.0 4.8 %all-to-all-done.1 = bf16[64,6,2048]{2,1,0:T(8,128)(2,1)} async-done(((bf16[64,6,2048]{2,1,0:T(8,128)(2,1)}), bf16[64,6,2048]{2,1,0:T(8,128)(2,1)}, u32[]{:S(2)}, u32[]{:S(2)}) %all-to-all-start.1) | async-done | bytes 1572896 | tf_op jit(solution)/shard_map/all_to_all | solution.py:137
  314.8 3.7 %reshape.173 = bf16[384,2048]{1,0:T(8,128)(2,1)} reshape(bf16[64,6,2048]{2,1,0:T(8,128)(2,1)} %all-to-all-done.1) | data formatting | bytes 3145728 | tf_op jit(solution)/shard_map/reshape | solution.py:144
  318.5 4.9 %gather_fusion.1 = bf16[256,2048]{1,0:T(8,128)(2,1)} fusion(bf16[384,2048]{1,0:T(8,128)(2,1)} %reshape.173, s32[1024]{0:T(1024)S(1)} %pad_clamp_fusion), kind=kCustom, calls=%fused_computation.1 | custom fusion | bytes 2098176 | tf_op jit(solution)/shard_map/gather | solution.py:144
  323.4 3.4 reshape.174
  326.8 5.8 %multiply_reduce_fusion = f32[128,2048]{1,0:T(8,128)} fusion(f32[128,2,2048]{2,1,0:T(2,128)} %reshape.174, f32[128,2]{1,0:T(8,128)S(1)} %copy.22), kind=kLoop, calls=%fused_computation.46 | loop fusion | flops 786432 | bytes 3146752 | tf_op jit(solution)/shard_map/reduce_sum | solution.py:146
  332.6 2.8 fusion.1
  (67 shorter events, 12.5 us)
Async XLA Ops:
  7.2 164.0 %copy-start = (bf16[1,512,2048]{2,1,0:T(8,128)(2,1)S(1)}, bf16[1,512,2048]{2,1,0:T(8,128)(2,1)}, u32[]{:S(2)}) copy-start(bf16[1,512,2048]{2,1,0:T(8,128)(2,1)} %param.22) | copy-start | bytes 6291460
  7.2 5.8 %copy-start.1 = (bf16[128,2048]{1,0:T(8,128)(2,1)S(1)}, bf16[128,2048]{1,0:T(8,128)(2,1)}, u32[]{:S(2)}) copy-start(bf16[128,2048]{1,0:T(8,128)(2,1)} %param.18) | copy-start | bytes 1572868
  7.2 6.3 %copy-start.5 = (f32[2048]{0:T(1024)S(1)}, f32[2048]{0:T(1024)}, u32[]{:S(2)}) copy-start(f32[2048]{0:T(1024)} %param.19) | copy-start | bytes 24580
  7.2 155.4 %all-gather.6.cloned.1.call-start = ((), (), s32[]{:S(2)}) async-start(), calls=%async_computation.3 | async-start | bytes 7864320 | tf_op jit(solution)/shard_map/all_gather | solution.py:124
  96.7 153.8 %reduce-scatter.2.cloned.1.call-start = ((), (), s32[]{:S(2)}) async-start(), calls=%async_computation.4 | async-start | bytes 7864320 | tf_op jit(solution)/shard_map/reduce_scatter | solution.py:131
  183.0 1.0 copy-start.2
  183.0 3.8 %copy-start.4 = (f32[31,2048]{1,0:T(8,128)S(1)}, f32[31,2048]{1,0:T(8,128)}, u32[]{:S(2)}) copy-start(f32[31,2048]{1,0:T(8,128)} %param.15) | copy-start | bytes 761860
  183.0 13.6 %copy-start.6 = (f32[2048]{0:T(1024)S(1)}, f32[2048]{0:T(1024)}, u32[]{:S(2)}) copy-start(f32[2048]{0:T(1024)} %param.16) | copy-start | bytes 24580
  183.0 94.5 %all-gather.8.cloned.1.call-start = ((), (), s32[]{:S(2)}) async-start(), calls=%async_computation.5 | async-start | bytes 1310720 | tf_op jit(solution)/shard_map/all_gather | solution.py:28
  184.1 7.5 %collective-permute-start = (bf16[30,2048]{1,0:T(8,128)(2,1)S(1)}, bf16[30,2048]{1,0:T(8,128)(2,1)S(1)}, u32[]{:S(2)}, u32[]{:S(2)}) collective-permute-start(bf16[30,2048]{1,0:T(8,128)(2,1)S(1)} %slice.198), channel_id=1, source_target_pairs={{0,1},{1,2},{2,3},{3,4},{4,5},{5,6},{6,7},{7,8},{8,9},{9,10},{10,1... | collective-permute-start | bytes 368648 | tf_op jit(solution)/shard_map/ppermute | solution.py:12
  254.2 11.6 %copy-start.7 = (f32[128,2]{0,1:T(2,128)S(1)}, f32[128,2]{0,1:T(2,128)}, u32[]{:S(2)}) copy-start(f32[128,2]{0,1:T(2,128)} %param.27) | copy-start | bytes 3076
  254.2 11.7 %copy-start.8 = (bf16[2048,128]{1,0:T(8,128)(2,1)S(1)}, bf16[2048,128]{1,0:T(8,128)(2,1)}, u32[]{:S(2)}) copy-start(bf16[2048,128]{1,0:T(8,128)(2,1)} %param.23) | copy-start | bytes 1572868
  254.2 60.6 %all-to-all-start.1 = ((bf16[64,6,2048]{2,1,0:T(8,128)(2,1)}), bf16[64,6,2048]{2,1,0:T(8,128)(2,1)}, u32[]{:S(2)}, u32[]{:S(2)}) async-start(bf16[64,6,2048]{2,1,0:T(8,128)(2,1)} %reshape.172), calls=%async_computation.2 | async-start | bytes 4194304 | tf_op jit(solution)/shard_map/all_to_all | solution.py:137
  265.2 41.4 %all-gather.10.cloned.1.call-start = ((), (), s32[]{:S(2)}) async-start(), calls=%async_computation.6 | async-start | bytes 1310720 | tf_op jit(solution)/shard_map/all_gather | solution.py:28
  326.8 5.8 %copy-start.3 = (bf16[128,2048]{1,0:T(8,128)(2,1)S(1)}, bf16[128,2048]{1,0:T(8,128)(2,1)}, u32[]{:S(2)}) copy-start(bf16[128,2048]{1,0:T(8,128)(2,1)} %param.25) | copy-start | bytes 1572868
Sparse Core Ops, SparseCore 0:
  96.8 65.8 all-gather.5
  183.1 67.3 reduce-scatter.1
  252.9 24.6 all-gather.7
  279.8 26.7 all-gather.9
where the time goes:
time: 343 us; the launch traced here: 342 us
  waiting for transfers between devices  166 us (48%)
  blocking collectives  62.6 us (18%)
  local copies, waits for them, and re-layouts  39.2 us (11%)
  matrix products  28.7 us (8%)
  other arithmetic  17.5 us (5%)
  starting transfers between devices  14.3 us (4%)
  between operations  14.1 us (4%)
    all_gather x1, waiting for transfers between devices, on_device(): lax.all_gather(arrived.reshape(ep_ranks * slot_count, model_width), 'tp',...  65.7 us
    all_to_all x1, blocking collectives, on_device(): lax.all_to_all(own_rows, 'ep', split_axis=0, concat_axis=0, tiled=True)  62.6 us
    reduce_scatter x1, waiting for transfers between devices, on_device(): lax.psum_scatter(jnp.dot(row_piece, down_local, preferred_element_type=jn...  52.5 us
    all_gather x2, waiting for transfers between devices, on_gathered_pieces(): finished.append(jax.vmap(apply)(lax.all_gather(slab, axis), starts))  37.7 us
    gather x2, local copies, waits for them, and re-layouts, fill_slots(): picked = row_data[block_ids, slot_row]  13.1 us
    dot_general x1, matrix products, on_device(): jnp.dot(row_piece, down_local, preferred_element_type=jnp.float32)  11.8 us
    all_to_all x1, starting transfers between devices, on_device(): lax.all_to_all(summed.reshape(ep_ranks, slot_count, model_width), 'ep', s...  11 us
    dot_general x2, matrix products, gated(): jnp.dot(row_data, gate_weight, preferred_element_type=jnp.float32)  8.89 us
  transfers between devices with their start and end apart: 6, of which 6 were waited for; matrix products, arithmetic and copies ran while one was open for 5% of the time, Pallas kernels for 0%

commit v1 on v0

v1 whole, which is shorter than its diff:
```python
import functools

import jax
import jax.numpy as jnp
from jax import lax
from jax.experimental import pallas as pl
from jax.experimental.pallas import tpu as pltpu
from jax.sharding import PartitionSpec as P

NORM_EPS = 1e-05
BF = jnp.bfloat16
F32 = jnp.float32
MESH_ID = pl.DeviceIdType.MESH
NZ, NX, NC, NY = 8, 4, 2, 4
NU = NX * NC
SL = 6
SLP = 8
CH = NU * SL
ROWS = 16


def remote(src, dst, send, recv, ep, tp):
    return pltpu.make_async_remote_copy(
        src_ref=src,
        dst_ref=dst,
        send_sem=send,
        recv_sem=recv,
        device_id=(ep, tp),
        device_id_type=MESH_ID,
    )


def shift_of(k):
    half = lax.div(k, 2)
    odd = lax.rem(k, 2)
    return odd * lax.rem(half + 1, 4) + (1 - odd) * (7 - half)


def silu(a):
    return a * lax.logistic(a)


def scaled(values, gain):
    center = values - jnp.mean(values, axis=-1, keepdims=True)
    spread = jnp.mean(center * center, axis=-1, keepdims=True)
    return center * lax.rsqrt(spread + NORM_EPS) * gain


def dot(a, b):
    return jnp.dot(a, b, preferred_element_type=F32)


def body(
    conv_in,
    conv_k,
    conv_g,
    ow_hbm,
    moe_in,
    moe_g,
    gate_hbm,
    up_hbm,
    down_hbm,
    sgate,
    sup,
    sdown,
    index,
    weight,
    conv_out,
    moe_out,
    ow,
    gate,
    up,
    down,
    halo,
    cpad,
    mixed,
    normed,
    tok,
    code_own,
    code_all,
    select,
    disp,
    xin,
    hid,
    part,
    rsa,
    rsb,
    ret,
    back,
    xs,
    xr,
    pick,
    shared,
    ld,
    halo_sem,
    tx_s,
    tx_r,
    code_s,
    code_r,
    cv_s,
    cv_r,
    zd_s,
    zd_r,
    ag_s,
    ag_r,
    rs_s,
    rs_r,
    zr_s,
    zr_r,
    xr_s,
    xr_r,
):
    tokens, width = moe_in.shape
    half = width // 2
    low, high = pl.ds(0, half), pl.ds(half, half)
    ep = lax.axis_index("ep")
    y = lax.axis_index("tp")
    z, u = lax.div(ep, NU), lax.rem(ep, NU)
    x, c = lax.div(u, NC), lax.rem(u, NC)
    yp, ym, yo = lax.rem(y + 1, NY), lax.rem(y + NY - 1, NY), lax.rem(y + 2, NY)

    def at_zu(zz, uu):
        return zz * NU + uu

    def at_xc(xx, cc):
        return z * NU + lax.rem(xx + NX, NX) * NC + cc

    flat = ep * NY + y
    count = NZ * NU * NY
    ahead = lax.rem(flat + 1, count)
    behind = lax.rem(flat + count - 1, count)

    barrier = pltpu.get_barrier_semaphore()

    def greet(e, t):
        pl.semaphore_signal(barrier, inc=1, device_id=(e, t), device_id_type=MESH_ID)

    greet(ep, yp)
    greet(ep, ym)
    for d in range(1, NZ):
        greet(at_zu(lax.rem(z + d, NZ), u), y)
    for d in range(1, NU):
        greet(at_zu(z, lax.rem(u + d, NU)), y)
    greet(lax.div(ahead, NY), lax.rem(ahead, NY))
    greet(lax.div(behind, NY), lax.rem(behind, NY))

    loads = [
        pltpu.make_async_copy(gate_hbm.at[0], gate, ld.at[0]),
        pltpu.make_async_copy(up_hbm.at[0], up, ld.at[1]),
        pltpu.make_async_copy(down_hbm.at[0], down, ld.at[2]),
        pltpu.make_async_copy(ow_hbm, ow, ld.at[3]),
    ]
    for load in loads:
        load.start()

    def norm_rows(r, _):
        rows = pl.ds(pl.multiple_of(r * ROWS, ROWS), ROWS)
        tok[u, rows, :] = scaled(moe_in[rows, :].astype(F32), moe_g[...]).astype(BF)
        return 0

    lax.fori_loop(0, tokens // ROWS, norm_rows, 0)

    own_index = index[pl.ds(pl.multiple_of(y * tokens, tokens), tokens), :]
    lane = lax.broadcasted_iota(jnp.int32, (tokens, 128), 1)
    expert = jnp.where(lane < NZ * NU, (lane & (NZ - 1)) * NU + (lane >> 3), -1)
    first = own_index[:, 0:1] == expert
    second = own_index[:, 1:2] == expert
    named = (first | second).astype(F32).astype(BF)
    row_i = lax.broadcasted_iota(jnp.int32, (tokens, tokens), 0)
    col_i = lax.broadcasted_iota(jnp.int32, (tokens, tokens), 1)
    earlier = (row_i < col_i).astype(F32).astype(BF)
    same = (row_i == col_i).astype(F32).astype(BF)
    over_tokens = (((0,), (0,)), ((), ()))
    named_t = lax.dot_general(named, same, over_tokens, preferred_element_type=F32)
    rank_t = lax.dot_general(named, earlier, over_tokens, preferred_element_type=F32)
    offset = (u * SL).astype(F32)
    code = jnp.where(named_t > 0.5, rank_t + offset, -1.0)
    for v in range(NU):
        code_own[v] = code[v * NZ : (v + 1) * NZ, :]
    rank = dot((row_i > col_i).astype(F32).astype(BF), named)
    slot_first = jnp.sum(jnp.where(first, rank, 0.0), axis=1, keepdims=True)
    slot_second = jnp.sum(jnp.where(second, rank, 0.0), axis=1, keepdims=True)
    place_first = own_index[:, 0:1] * SLP + slot_first.astype(jnp.int32)
    place_second = own_index[:, 1:2] * SLP + slot_second.astype(jnp.int32)
    place = lax.broadcasted_iota(jnp.int32, (tokens, NZ * NU * SLP), 1)
    pick[0:tokens, :] = (place == place_first).astype(F32).astype(BF)
    pick[tokens : 2 * tokens, :] = (place == place_second).astype(F32).astype(BF)

    pl.semaphore_wait(barrier, NZ - 1 + NU - 1 + 4)

    halo_copy = remote(
        conv_in.at[pl.ds(tokens - 32, 32), :],
        halo,
        halo_sem.at[0],
        halo_sem.at[1],
        lax.div(ahead, NY),
        lax.rem(ahead, NY),
    )
    halo_copy.start()

    def code_copy(d):
        v = lax.rem(u + d, NU)
        return remote(
            code_own.at[v], code_all.at[u], code_s.at[d], code_r.at[d], at_zu(z, v), y
        )

    def tok_copy(n, slot, columns, to):
        where = tok.at[slot, :, columns]
        return remote(where, where, tx_s.at[n], tx_r.at[n], to, y)

    u_of = lambda xx: lax.rem(xx + NX, NX) * NC + c
    xp, xm, mate = at_xc(x + 1, c), at_xc(x - 1, c), at_xc(x, 1 - c)
    every = pl.ds(0, width)
    tok_sends = [
        tok_copy(0, u, every, xp),
        tok_copy(1, u, every, xm),
        tok_copy(2, u_of(x - 1), low, xp),
        tok_copy(3, u_of(x + 1), high, xm),
        tok_copy(4, u, every, mate),
        tok_copy(5, u_of(x - 1), every, mate),
        tok_copy(6, u_of(x + 1), every, mate),
        tok_copy(7, u_of(x + 2), every, mate),
    ]

    def tok_wait(n, slot, columns):
        tok_copy(n, slot, columns, mate).wait_recv()

    mate_u = lambda xx: lax.rem(xx + NX, NX) * NC + 1 - c

    tok_sends[0].start()
    tok_sends[1].start()
    tok_sends[4].start()
    for d in range(1, NU):
        code_copy(d).start()

    blocks = width // 128

    def fill(b, _):
        columns = pl.ds(pl.multiple_of(b * 128, 128), 128)
        cpad[b, 32 : 32 + tokens, :] = conv_in[:, columns].astype(F32)
        return 0

    lax.fori_loop(0, blocks, fill, 0)
    halo_copy.wait_recv()
    keep = jnp.where(flat == 0, 0.0, 1.0)
    taps = conv_k.shape[0]

    def convolve(b, _):
        columns = pl.ds(pl.multiple_of(b * 128, 128), 128)
        cpad[b, 0:32, :] = halo[:, columns].astype(F32) * keep
        total = jnp.zeros((tokens, 128), F32)
        for k in range(taps):
            start = 33 - taps + k
            total = total + cpad[b, start : start + tokens, :] * conv_k[k : k + 1, columns]
        mixed[:, columns] = total
        return 0

    lax.fori_loop(0, blocks, convolve, 0)

    def conv_norm(r, _):
        rows = pl.ds(pl.multiple_of(r * ROWS, ROWS), ROWS)
        normed[y, rows, :] = silu(scaled(mixed[rows, :], conv_g[...])).astype(BF)
        return 0

    lax.fori_loop(0, tokens // ROWS, conv_norm, 0)

    def conv_copy(n, slot, columns, to):
        where = normed.at[slot, :, columns]
        return remote(where, where, cv_s.at[n], cv_r.at[n], ep, to)

    conv_sends = [
        conv_copy(0, y, every, yp),
        conv_copy(1, y, every, ym),
        conv_copy(2, ym, low, yp),
        conv_copy(3, yp, high, ym),
    ]
    conv_sends[0].start()
    conv_sends[1].start()

    tok_wait(0, u_of(x - 1), every)
    tok_sends[2].start()
    tok_sends[5].start()
    tok_wait(1, u_of(x + 1), every)
    tok_sends[3].start()
    tok_sends[6].start()
    conv_copy(0, ym, every, yp).wait_recv()
    conv_sends[2].start()
    conv_copy(1, yp, every, ym).wait_recv()
    conv_sends[3].start()
    for d in range(1, NU):
        v = lax.rem(u + NU - d, NU)
        remote(
            code_own.at[v], code_all.at[v], code_s.at[d], code_r.at[d], at_zu(z, v), y
        ).wait_recv()
    code_all[u] = code_own[u]
    slot_row = lax.broadcasted_iota(jnp.int32, (CH, tokens), 0).astype(F32)

    def build(v, _):
        columns = pl.ds(pl.multiple_of(v * tokens, tokens), tokens)
        codes = code_all[v]
        for zz in range(NZ):
            hit = slot_row == codes[zz : zz + 1, :]
            select[zz * CH : (zz + 1) * CH, columns] = hit.astype(F32).astype(BF)
        return 0

    lax.fori_loop(0, NU, build, 0)
    tok_wait(2, u_of(x + 2), low)
    tok_wait(3, u_of(x + 2), high)
    tok_sends[7].start()
    tok_wait(4, mate_u(x), every)
    tok_wait(5, mate_u(x - 1), every)
    tok_wait(6, mate_u(x + 1), every)
    tok_wait(7, mate_u(x + 2), every)

    wide = 512

    def gather(b, _):
        columns = pl.ds(pl.multiple_of(b * wide, wide), wide)
        rows = dot(select[...], tok[:, :, columns].reshape(NU * tokens, wide))
        disp[:, :, columns] = rows.astype(BF).reshape(NZ, CH, wide)
        return 0

    lax.fori_loop(0, width // wide, gather, 0)

    def disp_copy(k):
        target = lax.rem(z + shift_of(k), NZ)
        return remote(
            disp.at[target], xin.at[k, y], zd_s.at[k], zd_r.at[k], at_zu(target, u), y
        )

    def send_disp(k, _):
        disp_copy(k).start()
        return 0

    lax.fori_loop(0, NZ - 1, send_disp, 0)
    xin[NZ - 1, y] = disp[z]
    for load in loads:
        load.wait()

    def ag_copy(k, n, slot, columns, to):
        where = xin.at[k, slot, :, columns]
        return remote(where, where, ag_s.at[k, n], ag_r.at[k, n], ep, to)

    def ag_sends(k):
        return [
            ag_copy(k, 0, y, every, yp),
            ag_copy(k, 1, y, every, ym),
            ag_copy(k, 2, ym, low, yp),
            ag_copy(k, 3, yp, high, ym),
        ]

    def rs_sends(k):
        return [
            remote(part.at[k, yo, :, low], rsa.at[k, 0], rs_s.at[k, 0], rs_r.at[k, 0], ep, yp),
            remote(part.at[k, yo, :, high], rsa.at[k, 1], rs_s.at[k, 1], rs_r.at[k, 1], ep, ym),
            remote(part.at[k, yp], rsb.at[k, 0], rs_s.at[k, 2], rs_r.at[k, 2], ep, yp),
            remote(part.at[k, ym], rsb.at[k, 1], rs_s.at[k, 3], rs_r.at[k, 3], ep, ym),
        ]

    def ret_copy(k):
        source = lax.rem(z - shift_of(k) + NZ, NZ)
        return remote(ret.at[k], back.at[k], zr_s.at[k], zr_r.at[k], at_zu(source, u), y)

    def xr_copy(k, d):
        zz = lax.rem(z + shift_of(k), NZ)
        v = lax.rem(u + d, NU)
        return remote(
            xs.at[k, v], xr.at[zz, u], xr_s.at[k, d], xr_r.at[k, d], at_zu(z, v), y
        )

    def rows_out(k):
        @pl.when(k < NZ - 1)
        def _():
            disp_copy(k).wait_recv()

        sends = ag_sends(k)
        sends[0].start()
        sends[1].start()

    def rows_on(k):
        sends = ag_sends(k)
        ag_copy(k, 0, ym, every, yp).wait_recv()
        sends[2].start()
        ag_copy(k, 1, yp, every, ym).wait_recv()
        sends[3].start()

    def experts(k):
        ag_copy(k, 2, yo, low, yp).wait_recv()
        ag_copy(k, 3, yo, high, ym).wait_recv()
        rows = xin[k].reshape(NY * CH, width)
        ff = gate.shape[1]
        for b in range(ff // 256):
            columns = slice(b * 256, (b + 1) * 256)
            hid[:, columns] = (silu(dot(rows, gate[:, columns])) * dot(rows, up[:, columns])).astype(BF)

        def project(b, _):
            columns = pl.ds(pl.multiple_of(b * wide, wide), wide)
            out = dot(hid[...], down[:, columns]).astype(BF)
            part[k, :, :, columns] = out.reshape(NY, CH, wide)
            return 0

        lax.fori_loop(0, width // wide, project, 0)
        sends = rs_sends(k)
        sends[0].start()
        sends[1].start()

    def parts_on(k):
        sends = rs_sends(k)
        sends[0].wait_recv()
        kept = part[k, yp, :, low].astype(F32) + rsa[k, 0].astype(F32)
        part[k, yp, :, low] = kept.astype(BF)
        sends[2].start()
        sends[1].wait_recv()
        kept = part[k, ym, :, high].astype(F32) + rsa[k, 1].astype(F32)
        part[k, ym, :, high] = kept.astype(BF)
        sends[3].start()

    def results(k):
        sends = rs_sends(k)
        sends[2].wait_recv()
        sends[3].wait_recv()
        total = part[k, y].astype(F32) + rsb[k, 0].astype(F32) + rsb[k, 1].astype(F32)
        total = total.astype(BF)

        @pl.when(k < NZ - 1)
        def _():
            ret[k] = total
            ret_copy(k).start()

        @pl.when(k == NZ - 1)
        def _():
            back[k] = total

    spread_r = lax.broadcasted_iota(jnp.int32, (NU * SLP, CH), 0)
    spread_c = lax.broadcasted_iota(jnp.int32, (NU * SLP, CH), 1)
    spread = ((spread_r & 7) < SL) & (spread_c == (spread_r >> 3) * SL + (spread_r & 7))
    spread = spread.astype(F32).astype(BF)

    def results_home(k):
        @pl.when(k < NZ - 1)
        def _():
            ret_copy(k).wait_recv()

        def widen(b, _):
            columns = pl.ds(pl.multiple_of(b * wide, wide), wide)
            out = dot(spread, back[k, :, columns])
            xs[k, :, :, columns] = out.reshape(NU, SLP, wide).astype(BF)
            return 0

        lax.fori_loop(0, width // wide, widen, 0)

        def send(d, _):
            xr_copy(k, d).start()
            return 0

        lax.fori_loop(1, NU, send, 0)
        xr[lax.rem(z + shift_of(k), NZ), u] = xs[k, u]

    def beside():
        own = tok[u]
        hidden = (silu(dot(own, sgate[...])) * dot(own, sup[...])).astype(BF)
        shared[...] = dot(hidden, sdown[...])
        conv_copy(2, yo, low, yp).wait_recv()
        conv_copy(3, yo, high, ym).wait_recv()

        def project(b, _):
            rows = pl.ds(pl.multiple_of(b * tokens, tokens), tokens)
            conv_out[rows, :] = dot(normed[b], ow[...]).astype(BF)
            return 0

        lax.fori_loop(0, NY, project, 0)

    def stage(i, lag, act):
        k = i - lag

        @pl.when((k >= 0) & (k < NZ))
        def _():
            act(k)

    def step(i, _):
        stage(i, 0, rows_out)
        stage(i, 1, rows_on)
        stage(i, 2, experts)
        stage(i, 3, parts_on)
        stage(i, 4, results)
        stage(i, 5, results_home)

        @pl.when(i == 0)
        def _():
            beside()

        return 0

    lax.fori_loop(0, NZ + 5, step, 0)

    def arrived(k, _):
        zz = lax.rem(z + shift_of(k), NZ)

        def one(d, _):
            v = lax.rem(u + NU - d, NU)
            remote(
                xs.at[k, v], xr.at[zz, v], xr_s.at[k, d], xr_r.at[k, d], at_zu(z, v), y
            ).wait_recv()
            return 0

        lax.fori_loop(1, NU, one, 0)
        return 0

    lax.fori_loop(0, NZ, arrived, 0)

    def combine(b, _):
        columns = pl.ds(pl.multiple_of(b * wide, wide), wide)
        rows = xr[:, :, :, columns].astype(F32).reshape(NZ * NU * SLP, wide).astype(BF)
        both = dot(pick[...], rows)
        routed = both[0:tokens] * weight[:, 0:1] + both[tokens : 2 * tokens] * weight[:, 1:2]
        moe_out[:, columns] = (shared[:, columns] + routed).astype(BF)
        return 0

    lax.fori_loop(0, width // wide, combine, 0)

    halo_copy.wait_send()
    for copy in tok_sends + conv_sends:
        copy.wait_send()
    for d in range(1, NU):
        code_copy(d).wait_send()

    def drained(k, _):
        @pl.when(k < NZ - 1)
        def _():
            disp_copy(k).wait_send()
            ret_copy(k).wait_send()

        for copy in ag_sends(k) + rs_sends(k):
            copy.wait_send()

        def one(d, _):
            xr_copy(k, d).wait_send()
            return 0

        lax.fori_loop(1, NU, one, 0)
        return 0

    lax.fori_loop(0, NZ, drained, 0)


def on_device(*args):
    (
        conv_input,
        conv_kernel,
        conv_gain,
        out_weight,
        moe_input,
        moe_gain,
        expert_gate,
        expert_up,
        expert_down,
        shared_gate,
        shared_up,
        shared_down,
        expert_index,
        routing_weight,
    ) = args
    tokens, width = moe_input.shape
    half = width // 2
    ff = expert_gate.shape[2]
    cols = out_weight.shape[1]
    vm = lambda *shape, dtype=BF: pltpu.VMEM(shape, dtype)
    dma = lambda *shape: pltpu.SemaphoreType.DMA(shape)
    in_vmem = pl.BlockSpec(memory_space=pltpu.VMEM)
    in_hbm = pl.BlockSpec(memory_space=pl.ANY)
    operands = (
        (conv_input, in_vmem),
        (conv_kernel, in_vmem),
        (conv_gain.reshape(1, width), in_vmem),
        (out_weight, in_hbm),
        (moe_input, in_vmem),
        (moe_gain.reshape(1, width), in_vmem),
        (expert_gate, in_hbm),
        (expert_up, in_hbm),
        (expert_down, in_hbm),
        (shared_gate, in_vmem),
        (shared_up, in_vmem),
        (shared_down, in_vmem),
        (expert_index, in_vmem),
        (routing_weight, in_vmem),
    )
    scratch = [
        vm(width, cols),
        vm(width, ff),
        vm(width, ff),
        vm(ff, width),
        vm(32, width),
        vm(width // 128, 32 + tokens, 128, dtype=F32),
        vm(tokens, width, dtype=F32),
        vm(NY, tokens, width),
        vm(NU, tokens, width),
        vm(NU, NZ, tokens, dtype=F32),
        vm(NU, NZ, tokens, dtype=F32),
        vm(NZ * CH, NU * tokens),
        vm(NZ, CH, width),
        vm(NZ, NY, CH, width),
        vm(NY * CH, ff),
        vm(NZ, NY, CH, width),
        vm(NZ, 2, CH, half),
        vm(NZ, 2, CH, width),
        vm(NZ, CH, width),
        vm(NZ, CH, width),
        vm(NZ, NU, SLP, width),
        vm(NZ, NU, SLP, width),
        vm(2 * tokens, NZ * NU * SLP),
        vm(tokens, width, dtype=F32),
        dma(4),
        dma(2),
        dma(8),
        dma(8),
        dma(NU),
        dma(NU),
        dma(4),
        dma(4),
        dma(NZ),
        dma(NZ),
        dma(NZ, 4),
        dma(NZ, 4),
        dma(NZ, 4),
        dma(NZ, 4),
        dma(NZ),
        dma(NZ),
        dma(NZ, NU),
        dma(NZ, NU),
    ]
    return pl.pallas_call(
        body,
        out_shape=(
            jax.ShapeDtypeStruct((NY * tokens, cols), BF),
            jax.ShapeDtypeStruct((tokens, width), BF),
        ),
        in_specs=[spec for _, spec in operands],
        out_specs=(in_vmem, in_vmem),
        scratch_shapes=scratch,
        compiler_params=pltpu.CompilerParams(
            collective_id=0, has_side_effects=True, vmem_limit_bytes=67043328
        ),
    )(*[array for array, _ in operands])


def solution(mesh):
    in_specs = (
        P(("ep", "tp"), None),
        P(),
        P(),
        P(None, "tp"),
        P(("ep", "tp"), None),
        P(),
        P("ep", None, "tp"),
        P("ep", None, "tp"),
        P("ep", "tp", None),
        P(),
        P(),
        P(),
        P("ep", None),
        P(("ep", "tp"), None),
    )
    out_specs = (P("ep", "tp"), P(("ep", "tp"), None))
    return jax.shard_map(
        on_device, mesh=mesh, in_specs=in_specs, out_specs=out_specs, check_vma=False
    )
```

time: 343 us -> 184 us (0.54)
  the two profiles are of different devices: /device:TPU:1 before, /device:TPU:37 now
where the time goes in v1:
time: 184 us
  Pallas kernels  176 us (96%)
  local copies, waits for them, and re-layouts  6.7 us (4%)
    pallas_call x1, Pallas kernels, on_device(): pl.pallas_call(body, out_shape=(jax.ShapeDtypeStruct((NY * tokens, cols),...  176 us
    unnamed x4, local copies, waits for them, and re-layouts  6.7 us

profile of v1, /device:TPU:37, one launch (start us, length us, event | category | flops | bytes accessed | tf_op | source)
XLA Modules:
  0.0 183.5 jit_solution(235369205644269445)
XLA Ops:
  0.6 1.4 copy.17.weight
  2.0 1.5 copy.16.index
  3.6 176.2 %shard_map.149 = (bf16[512,512]{1,0:T(8,128)(2,1)}, bf16[128,2048]{1,0:T(8,128)(2,1)}) custom-call(bf16[128,2048]{1,0:T(8,128)(2,1)} %conv_in.1, f32[31,2048]{1,0:T(8,128)} %conv_k.1, f32[1,2048]{1,0:T(1,128)} %bitcast.2, bf16[2048,512]{1,0:T(8,128)(2,1)} %ow_hbm.1, bf16[128,2048]{1,0:T(8,128)(2,1)} %moe_in.1, f32[1,2048]{1,0:T(1,128)} %bitcast.3, ...), custom_call_target="tpu_custom_call" | custom-call | tf_op jit(solution)/shard_map/pallas_call | solution.py:631
  179.8 1.9 %copy.20 = bf16[512,512]{1,0:T(8,128)(2,1)} copy(bf16[512,512]{1,0:T(8,128)(2,1)} %get-tuple-element.4) | data formatting | bytes 1048576
  181.6 1.9 %copy.21 = bf16[128,2048]{1,0:T(8,128)(2,1)} copy(bf16[128,2048]{1,0:T(8,128)(2,1)} %get-tuple-element.5) | data formatting | bytes 1048576

commit v2 on v1

v2 whole, which is shorter than its diff:
```python
import functools

import jax
import jax.numpy as jnp
from jax import lax
from jax.experimental import pallas as pl
from jax.experimental.pallas import tpu as pltpu
from jax.sharding import PartitionSpec as P

NORM_EPS = 1e-05
BF = jnp.bfloat16
F32 = jnp.float32
MESH_ID = pl.DeviceIdType.MESH
NZ, NU, NY = 8, 8, 4
SL = 6
SLP = 8
CH = NU * SL
ROWS = 16
EDGE = 32
HOME = 6
EARLY = 4


def remote(src, dst, send, recv, ep, tp):
    return pltpu.make_async_remote_copy(
        src_ref=src,
        dst_ref=dst,
        send_sem=send,
        recv_sem=recv,
        device_id=(ep, tp),
        device_id_type=MESH_ID,
    )


ORDER = (7, 2, 5, 3, 6, 4, 1, 0)
PACKED = sum(far << (4 * k) for k, far in enumerate(ORDER))


def shift_of(k):
    return lax.shift_right_logical(jnp.int32(PACKED), jnp.int32(4) * k) & 7


def silu(a):
    return a * lax.logistic(a)


def scaled(values, gain):
    center = values - jnp.mean(values, axis=-1, keepdims=True)
    spread = jnp.mean(center * center, axis=-1, keepdims=True)
    return center * lax.rsqrt(spread + NORM_EPS) * gain


def dot(a, b):
    return jnp.dot(a, b, preferred_element_type=F32)


def body(
    conv_hbm,
    taps_hbm,
    conv_g,
    ow_hbm,
    moe_hbm,
    moe_g,
    gate_hbm,
    up_hbm,
    down_hbm,
    sgate_hbm,
    sup_hbm,
    sdown_hbm,
    index,
    weight,
    conv_out,
    moe_out,
    conv_in,
    conv_k,
    moe_in,
    ow,
    gate,
    up,
    down,
    sgate,
    sup,
    sdown,
    halo,
    cpad,
    mixed,
    normed,
    own,
    xd,
    xdr,
    disp,
    xin,
    hid,
    part,
    rsa,
    rsb,
    ret,
    back,
    xs,
    xr,
    pick,
    shared,
    weights,
    ld,
    halo_sem,
    xd_s,
    xd_r,
    cv_s,
    cv_r,
    zd_s,
    zd_r,
    ag_s,
    ag_r,
    rs_s,
    rs_r,
    zr_s,
    zr_r,
    xr_s,
    xr_r,
):
    tokens, width = moe_in.shape
    half = width // 2
    wide = 512
    every, low, high = pl.ds(0, width), pl.ds(0, half), pl.ds(half, half)
    ep = lax.axis_index("ep")
    y = lax.axis_index("tp")
    z, u = lax.div(ep, NU), lax.rem(ep, NU)
    yp, ym, yo = lax.rem(y + 1, NY), lax.rem(y + NY - 1, NY), lax.rem(y + 2, NY)

    def at_zu(zz, uu):
        return zz * NU + uu

    flat = ep * NY + y
    count = NZ * NU * NY
    ahead = lax.rem(flat + 1, count)
    behind = lax.rem(flat + count - 1, count)

    barrier = pltpu.get_barrier_semaphore()

    def greet(e, t):
        pl.semaphore_signal(barrier, inc=1, device_id=(e, t), device_id_type=MESH_ID)

    greet(ep, yp)
    greet(ep, ym)
    for d in range(1, NZ):
        greet(at_zu(lax.rem(z + d, NZ), u), y)
    for d in range(1, NU):
        greet(at_zu(z, lax.rem(u + d, NU)), y)
    greet(lax.div(ahead, NY), lax.rem(ahead, NY))
    greet(lax.div(behind, NY), lax.rem(behind, NY))

    loads = [
        pltpu.make_async_copy(source, target, ld.at[n])
        for n, (source, target) in enumerate(
            (
                (moe_hbm, moe_in),
                (conv_hbm, conv_in),
                (taps_hbm, conv_k),
                (gate_hbm.at[0], gate),
                (up_hbm.at[0], up),
                (down_hbm.at[0], down),
                (ow_hbm, ow),
                (sgate_hbm, sgate),
                (sup_hbm, sup),
                (sdown_hbm, sdown),
            )
        )
    ]
    for load in loads:
        load.start()

    mine = index[:, pl.ds(pl.multiple_of(y * tokens, tokens), tokens)]
    expert = lax.broadcasted_iota(jnp.int32, (NZ * NU, tokens), 0)
    first = expert == mine[0:1, :]
    second = expert == mine[1:2, :]
    named = (first | second).astype(F32).astype(BF)
    row_i = lax.broadcasted_iota(jnp.int32, (tokens, tokens), 0)
    col_i = lax.broadcasted_iota(jnp.int32, (tokens, tokens), 1)
    rank = dot(named, (row_i < col_i).astype(F32).astype(BF))
    rank_first = jnp.sum(jnp.where(first, rank, 0.0), axis=0, keepdims=True)
    rank_second = jnp.sum(jnp.where(second, rank, 0.0), axis=0, keepdims=True)
    place_first = mine[0:1, :] * SLP + rank_first.astype(jnp.int32)
    place_second = mine[1:2, :] * SLP + rank_second.astype(jnp.int32)
    place = lax.broadcasted_iota(jnp.int32, (NZ * NU * SLP, tokens), 0)
    select = ((place == place_first) | (place == place_second)).astype(F32).astype(BF)

    share = weight[...]
    share_a = share.astype(BF).astype(F32)
    share_b = (share - share_a).astype(BF).astype(F32)
    share_c = share - share_a - share_b
    line = lax.broadcasted_iota(jnp.int32, (16, tokens), 0)
    table = jnp.zeros((16, tokens), F32)
    for n, values in enumerate(
        (
            mine[0:1, :].astype(F32),
            mine[1:2, :].astype(F32),
            rank_first,
            rank_second,
            share_a[0:1, :],
            share_a[1:2, :],
            share_b[0:1, :],
            share_b[1:2, :],
            share_c[0:1, :],
            share_c[1:2, :],
        )
    ):
        table = jnp.where(line == n, values, table)
    turned = lax.dot_general(
        (row_i == col_i).astype(F32).astype(BF),
        table.astype(BF),
        (((1,), (1,)), ((), ())),
        preferred_element_type=F32,
    )
    weights[:, 0:2] = turned[:, 4:6] + turned[:, 6:8] + turned[:, 8:10]
    places = (turned[:, 0:2] * SLP + turned[:, 2:4]).astype(jnp.int32)
    spot = lax.broadcasted_iota(jnp.int32, (tokens, NZ * NU * SLP), 1)
    pick[0:tokens, :] = (spot == places[:, 0:1]).astype(F32).astype(BF)
    pick[tokens : 2 * tokens, :] = (spot == places[:, 1:2]).astype(F32).astype(BF)

    loads[0].wait()

    def norm_rows(r, _):
        rows = pl.ds(pl.multiple_of(r * ROWS, ROWS), ROWS)
        own[rows, :] = scaled(moe_in[rows, :].astype(F32), moe_g[...]).astype(BF)
        return 0

    lax.fori_loop(0, tokens // ROWS, norm_rows, 0)

    def gather(b, _):
        columns = pl.ds(pl.multiple_of(b * wide, wide), wide)
        rows = dot(select, own[:, columns])
        xd[:, :, :, columns] = rows.reshape(NZ, NU, SLP, wide).astype(BF)
        return 0

    lax.fori_loop(0, width // wide, gather, 0)

    blocks = width // 128
    taps = conv_k.shape[0]
    loads[1].wait()
    loads[2].wait()

    def fill(b, _):
        columns = pl.ds(pl.multiple_of(b * 128, 128), 128)
        cpad[b, EDGE : EDGE + tokens, :] = conv_in[:, columns].astype(F32)
        return 0

    lax.fori_loop(0, blocks, fill, 0)

    def convolve(begin, length):
        def one(b, _):
            columns = pl.ds(pl.multiple_of(b * 128, 128), 128)
            total = jnp.zeros((length, 128), F32)
            for k in range(taps):
                start = begin + EDGE + 1 - taps + k
                total = total + cpad[b, start : start + length, :] * conv_k[k : k + 1, columns]
            mixed[begin : begin + length, columns] = total
            return 0

        lax.fori_loop(0, blocks, one, 0)

        def conv_norm(r, _):
            rows = pl.ds(pl.multiple_of(begin + r * ROWS, ROWS), ROWS)
            normed[y, rows, :] = silu(scaled(mixed[rows, :], conv_g[...])).astype(BF)
            return 0

        lax.fori_loop(0, length // ROWS, conv_norm, 0)

    def conv_copy(n, slot, columns, to):
        rows = pl.ds(EDGE, tokens - EDGE) if n < 4 else pl.ds(0, EDGE)
        where = normed.at[slot, rows, columns]
        return remote(where, where, cv_s.at[n], cv_r.at[n], ep, to)

    conv_sends = [
        conv_copy(0, y, every, yp),
        conv_copy(1, y, every, ym),
        conv_copy(2, ym, low, yp),
        conv_copy(3, yp, high, ym),
        conv_copy(4, y, every, yp),
        conv_copy(5, y, every, ym),
        conv_copy(6, ym, low, yp),
        conv_copy(7, yp, high, ym),
    ]
    convolve(EDGE, tokens - EDGE)

    pl.semaphore_wait(barrier, NZ - 1 + NU - 1 + 4)

    halo_copy = remote(
        conv_in.at[pl.ds(tokens - EDGE, EDGE), :],
        halo,
        halo_sem.at[0],
        halo_sem.at[1],
        lax.div(ahead, NY),
        lax.rem(ahead, NY),
    )
    halo_copy.start()

    def xd_copy(k, d):
        zz = lax.rem(z + shift_of(k), NZ)
        v = lax.rem(u + d, NU)
        return remote(
            xd.at[zz, v], xdr.at[zz, u], xd_s.at[k, d], xd_r.at[k, d], at_zu(z, v), y
        )

    def send_rows(k, _):
        def one(d, _):
            xd_copy(k, d).start()
            return 0

        return lax.fori_loop(1, NU, one, 0)

    send_rows(0, 0)
    conv_sends[0].start()
    conv_sends[1].start()
    lax.fori_loop(1, NZ, send_rows, 0)

    halo_copy.wait_recv()
    keep = jnp.where(flat == 0, 0.0, 1.0)

    def fill_edge(b, _):
        columns = pl.ds(pl.multiple_of(b * 128, 128), 128)
        cpad[b, 0:EDGE, :] = halo[:, columns].astype(F32) * keep
        return 0

    lax.fori_loop(0, blocks, fill_edge, 0)
    convolve(0, EDGE)
    conv_sends[4].start()
    conv_sends[5].start()

    wide_r = lax.broadcasted_iota(jnp.int32, (NU * SLP, CH), 0)
    wide_c = lax.broadcasted_iota(jnp.int32, (NU * SLP, CH), 1)
    spread = ((wide_r & 7) < SL) & (wide_c == (wide_r >> 3) * SL + (wide_r & 7))
    spread = spread.astype(F32).astype(BF)
    pack_r = lax.broadcasted_iota(jnp.int32, (CH, NU * SLP), 0)
    pack_c = lax.broadcasted_iota(jnp.int32, (CH, NU * SLP), 1)
    pack = ((pack_c & 7) < SL) & (pack_r == (pack_c >> 3) * SL + (pack_c & 7))
    pack = pack.astype(F32).astype(BF)

    def disp_copy(k):
        target = lax.rem(z + shift_of(k), NZ)
        return remote(
            disp.at[k], xin.at[k, y], zd_s.at[k], zd_r.at[k], at_zu(target, u), y
        )

    def rows_along(k):
        zz = lax.rem(z + shift_of(k), NZ)

        def one(d, _):
            v = lax.rem(u + NU - d, NU)
            remote(
                xd.at[zz, v], xdr.at[zz, v], xd_s.at[k, d], xd_r.at[k, d], at_zu(z, v), y
            ).wait_recv()
            return 0

        lax.fori_loop(1, NU, one, 0)
        xdr[zz, u] = xd[zz, u]

        def narrow(b, _):
            columns = pl.ds(pl.multiple_of(b * wide, wide), wide)
            rows = xdr[zz, :, :, columns].astype(F32).reshape(NU * SLP, wide).astype(BF)
            rows = dot(pack, rows).astype(BF)

            @pl.when(k < NZ - 1)
            def _():
                disp[k, :, columns] = rows

            @pl.when(k == NZ - 1)
            def _():
                xin[k, y, :, columns] = rows

            return 0

        lax.fori_loop(0, width // wide, narrow, 0)

        @pl.when(k < NZ - 1)
        def _():
            disp_copy(k).start()

    def rows_first(k, _):
        rows_along(k)
        return 0

    lax.fori_loop(0, 2, rows_first, 0)
    conv_copy(0, ym, every, yp).wait_recv()
    conv_sends[2].start()
    conv_copy(1, yp, every, ym).wait_recv()
    conv_sends[3].start()
    lax.fori_loop(2, 3, rows_first, 0)
    conv_copy(4, ym, every, yp).wait_recv()
    conv_sends[6].start()
    conv_copy(5, yp, every, ym).wait_recv()
    conv_sends[7].start()
    lax.fori_loop(3, EARLY, rows_first, 0)
    for load in loads[3:]:
        load.wait()

    def ag_copy(k, n, slot, columns, to):
        where = xin.at[k, slot, :, columns]
        return remote(where, where, ag_s.at[k, n], ag_r.at[k, n], ep, to)

    def ag_sends(k):
        return [
            ag_copy(k, 0, y, every, yp),
            ag_copy(k, 1, y, every, ym),
            ag_copy(k, 2, ym, low, yp),
            ag_copy(k, 3, yp, high, ym),
        ]

    def rs_sends(k):
        return [
            remote(part.at[k, yo, :, low], rsa.at[k, 0], rs_s.at[k, 0], rs_r.at[k, 0], ep, yp),
            remote(part.at[k, yo, :, high], rsa.at[k, 1], rs_s.at[k, 1], rs_r.at[k, 1], ep, ym),
            remote(part.at[k, yp], rsb.at[k, 0], rs_s.at[k, 2], rs_r.at[k, 2], ep, yp),
            remote(part.at[k, ym], rsb.at[k, 1], rs_s.at[k, 3], rs_r.at[k, 3], ep, ym),
        ]

    def ret_copy(k):
        source = lax.rem(z - shift_of(k) + NZ, NZ)
        return remote(ret.at[k], back.at[k], zr_s.at[k], zr_r.at[k], at_zu(source, u), y)

    def xr_copy(k, d):
        zz = lax.rem(z + shift_of(k), NZ)
        v = lax.rem(u + d, NU)
        return remote(
            xs.at[k, v], xr.at[zz, u], xr_s.at[k, d], xr_r.at[k, d], at_zu(z, v), y
        )

    def rows_out(k):
        @pl.when(k < NZ - 1)
        def _():
            disp_copy(k).wait_recv()

        sends = ag_sends(k)
        sends[0].start()
        sends[1].start()

    def rows_on(k):
        sends = ag_sends(k)
        ag_copy(k, 0, ym, every, yp).wait_recv()
        sends[2].start()
        ag_copy(k, 1, yp, every, ym).wait_recv()
        sends[3].start()

    def experts(k):
        ag_copy(k, 2, yo, low, yp).wait_recv()
        ag_copy(k, 3, yo, high, ym).wait_recv()
        rows = xin[k].reshape(NY * CH, width)
        ff = gate.shape[1]
        for b in range(ff // 256):
            columns = slice(b * 256, (b + 1) * 256)
            hid[:, columns] = (silu(dot(rows, gate[:, columns])) * dot(rows, up[:, columns])).astype(BF)

        def project(b, _):
            columns = pl.ds(pl.multiple_of(b * wide, wide), wide)
            out = dot(hid[...], down[:, columns]).astype(BF)
            part[k, :, :, columns] = out.reshape(NY, CH, wide)
            return 0

        lax.fori_loop(0, width // wide, project, 0)
        sends = rs_sends(k)
        sends[0].start()
        sends[1].start()

    def parts_on(k):
        sends = rs_sends(k)
        sends[0].wait_recv()
        kept = part[k, yp, :, low].astype(F32) + rsa[k, 0].astype(F32)
        part[k, yp, :, low] = kept.astype(BF)
        sends[2].start()
        sends[1].wait_recv()
        kept = part[k, ym, :, high].astype(F32) + rsa[k, 1].astype(F32)
        part[k, ym, :, high] = kept.astype(BF)
        sends[3].start()

    def results(k):
        sends = rs_sends(k)
        sends[2].wait_recv()
        sends[3].wait_recv()
        total = part[k, y].astype(F32) + rsb[k, 0].astype(F32) + rsb[k, 1].astype(F32)
        total = total.astype(BF)

        @pl.when(k < NZ - 1)
        def _():
            ret[k] = total
            ret_copy(k).start()

        @pl.when(k == NZ - 1)
        def _():
            back[k] = total

    def results_home(k):
        @pl.when(k < NZ - 1)
        def _():
            ret_copy(k).wait_recv()

        def widen(b, _):
            columns = pl.ds(pl.multiple_of(b * wide, wide), wide)
            out = dot(spread, back[k, :, columns])
            xs[k, :, :, columns] = out.reshape(NU, SLP, wide).astype(BF)
            return 0

        lax.fori_loop(0, width // wide, widen, 0)

        def send(d, _):
            xr_copy(k, d).start()
            return 0

        lax.fori_loop(1, NU, send, 0)
        xr[lax.rem(z + shift_of(k), NZ), u] = xs[k, u]

    def beside():
        rows = own[...]
        hidden = (silu(dot(rows, sgate[...])) * dot(rows, sup[...])).astype(BF)
        shared[...] = dot(hidden, sdown[...])
        conv_copy(2, yo, low, yp).wait_recv()
        conv_copy(3, yo, high, ym).wait_recv()
        conv_copy(6, yo, low, yp).wait_recv()
        conv_copy(7, yo, high, ym).wait_recv()

        def project(b, _):
            rows = pl.ds(pl.multiple_of(b * tokens, tokens), tokens)
            conv_out[rows, :] = dot(normed[b], ow[...]).astype(BF)
            return 0

        lax.fori_loop(0, NY, project, 0)

    def stage(i, lag, act):
        k = i - lag

        @pl.when((k >= 0) & (k < NZ))
        def _():
            act(k)

    def step(i, _):
        stage(i, 0, rows_out)
        stage(i, 1, rows_on)
        stage(i, 2, experts)
        stage(i, 3, parts_on)
        stage(i, 4, results)
        stage(i, -EARLY, rows_along)
        stage(i, HOME, results_home)

        @pl.when(i == 1)
        def _():
            beside()

        return 0

    lax.fori_loop(0, NZ + HOME, step, 0)

    def arrived(k, _):
        zz = lax.rem(z + shift_of(k), NZ)

        def one(d, _):
            v = lax.rem(u + NU - d, NU)
            remote(
                xs.at[k, v], xr.at[zz, v], xr_s.at[k, d], xr_r.at[k, d], at_zu(z, v), y
            ).wait_recv()
            return 0

        lax.fori_loop(1, NU, one, 0)
        return 0

    lax.fori_loop(0, NZ, arrived, 0)

    def combine(b, _):
        columns = pl.ds(pl.multiple_of(b * wide, wide), wide)
        rows = xr[:, :, :, columns].astype(F32).reshape(NZ * NU * SLP, wide).astype(BF)
        both = dot(pick[...], rows)
        routed = both[0:tokens] * weights[:, 0:1] + both[tokens : 2 * tokens] * weights[:, 1:2]
        moe_out[:, columns] = (shared[:, columns] + routed).astype(BF)
        return 0

    lax.fori_loop(0, width // wide, combine, 0)

    halo_copy.wait_send()
    for copy in conv_sends:
        copy.wait_send()

    def drained(k, _):
        @pl.when(k < NZ - 1)
        def _():
            disp_copy(k).wait_send()
            ret_copy(k).wait_send()

        for copy in ag_sends(k) + rs_sends(k):
            copy.wait_send()

        def one(d, _):
            xd_copy(k, d).wait_send()
            xr_copy(k, d).wait_send()
            return 0

        lax.fori_loop(1, NU, one, 0)
        return 0

    lax.fori_loop(0, NZ, drained, 0)


def on_device(*args):
    (
        conv_input,
        conv_kernel,
        conv_gain,
        out_weight,
        moe_input,
        moe_gain,
        expert_gate,
        expert_up,
        expert_down,
        shared_gate,
        shared_up,
        shared_down,
        expert_index,
        routing_weight,
    ) = args
    tokens, width = moe_input.shape
    half = width // 2
    ff = expert_gate.shape[2]
    cols = out_weight.shape[1]
    vm = lambda *shape, dtype=BF: pltpu.VMEM(shape, dtype)
    dma = lambda *shape: pltpu.SemaphoreType.DMA(shape)
    in_vmem = pl.BlockSpec(memory_space=pltpu.VMEM)
    in_hbm = pl.BlockSpec(memory_space=pl.ANY)
    operands = (
        (conv_input, in_hbm),
        (conv_kernel, in_hbm),
        (conv_gain.reshape(1, width), in_vmem),
        (out_weight, in_hbm),
        (moe_input, in_hbm),
        (moe_gain.reshape(1, width), in_vmem),
        (expert_gate, in_hbm),
        (expert_up, in_hbm),
        (expert_down, in_hbm),
        (shared_gate, in_hbm),
        (shared_up, in_hbm),
        (shared_down, in_hbm),
        (expert_index.T, in_vmem),
        (routing_weight.T, in_vmem),
    )
    scratch = [
        vm(tokens, width),
        vm(*conv_kernel.shape, dtype=F32),
        vm(tokens, width),
        vm(width, cols),
        vm(width, ff),
        vm(width, ff),
        vm(ff, width),
        vm(*shared_gate.shape),
        vm(*shared_up.shape),
        vm(*shared_down.shape),
        vm(EDGE, width),
        vm(width // 128, EDGE + tokens, 128, dtype=F32),
        vm(tokens, width, dtype=F32),
        vm(NY, tokens, width),
        vm(tokens, width),
        vm(NZ, NU, SLP, width),
        vm(NZ, NU, SLP, width),
        vm(NZ, CH, width),
        vm(NZ, NY, CH, width),
        vm(NY * CH, ff),
        vm(NZ, NY, CH, width),
        vm(NZ, 2, CH, half),
        vm(NZ, 2, CH, width),
        vm(NZ, CH, width),
        vm(NZ, CH, width),
        vm(NZ, NU, SLP, width),
        vm(NZ, NU, SLP, width),
        vm(2 * tokens, NZ * NU * SLP),
        vm(tokens, width, dtype=F32),
        vm(tokens, 128, dtype=F32),
        dma(10),
        dma(2),
        dma(NZ, NU),
        dma(NZ, NU),
        dma(8),
        dma(8),
        dma(NZ),
        dma(NZ),
        dma(NZ, 4),
        dma(NZ, 4),
        dma(NZ, 4),
        dma(NZ, 4),
        dma(NZ),
        dma(NZ),
        dma(NZ, NU),
        dma(NZ, NU),
    ]
    return pl.pallas_call(
        body,
        out_shape=(
            jax.ShapeDtypeStruct((NY * tokens, cols), BF),
            jax.ShapeDtypeStruct((tokens, width), BF),
        ),
        in_specs=[spec for _, spec in operands],
        out_specs=(in_vmem, in_vmem),
        scratch_shapes=scratch,
        compiler_params=pltpu.CompilerParams(
            collective_id=0, has_side_effects=True, vmem_limit_bytes=67043328
        ),
    )(*[array for array, _ in operands])


def solution(mesh):
    in_specs = (
        P(("ep", "tp"), None),
        P(),
        P(),
        P(None, "tp"),
        P(("ep", "tp"), None),
        P(),
        P("ep", None, "tp"),
        P("ep", None, "tp"),
        P("ep", "tp", None),
        P(),
        P(),
        P(),
        P("ep", None),
        P(("ep", "tp"), None),
    )
    out_specs = (P("ep", "tp"), P(("ep", "tp"), None))
    return jax.shard_map(
        on_device, mesh=mesh, in_specs=in_specs, out_specs=out_specs, check_vma=False
    )
```

time: 184 us -> 163 us (0.89)
  the two profiles are of different devices: /device:TPU:37 before, /device:TPU:1 now
where the time goes in v2:
time: 163 us; the launch traced here: 161 us
  Pallas kernels  157 us (96%)
  local copies, waits for them, and re-layouts  3.75 us (2%)
    pallas_call x1, Pallas kernels, on_device(): pl.pallas_call(body, out_shape=(jax.ShapeDtypeStruct((NY * tokens, cols),...  157 us
    unnamed x2, local copies, waits for them, and re-layouts  3.75 us

profile of v2, /device:TPU:1, one launch (start us, length us, event | category | flops | bytes accessed | tf_op | source)
XLA Modules:
  0.0 161.1 jit_solution(14761538933686336139)
XLA Ops:
  0.6 156.7 %shard_map.149 = (bf16[512,512]{1,0:T(8,128)(2,1)}, bf16[128,2048]{1,0:T(8,128)(2,1)}) custom-call(bf16[128,2048]{1,0:T(8,128)(2,1)} %conv_hbm.1, f32[31,2048]{1,0:T(8,128)} %taps_hbm.1, f32[1,2048]{1,0:T(1,128)} %bitcast.4, bf16[2048,512]{1,0:T(8,128)(2,1)} %ow_hbm.1, bf16[128,2048]{1,0:T(8,128)(2,1)} %moe_hbm.1, f32[1,2048]{1,0:T(1,128)} %bitcast.5, ...), custom_call_target="tpu_custom_call" | custom-call | tf_op jit(solution)/shard_map/pallas_call | solution.py:688
  157.3 1.9 %copy.18 = bf16[512,512]{1,0:T(8,128)(2,1)} copy(bf16[512,512]{1,0:T(8,128)(2,1)} %get-tuple-element.4) | data formatting | bytes 1048576
  159.2 1.9 %copy.19 = bf16[128,2048]{1,0:T(8,128)(2,1)} copy(bf16[128,2048]{1,0:T(8,128)(2,1)} %get-tuple-element.5) | data formatting | bytes 1048576

commit v3 on v2

v3 whole, which is shorter than its diff:
```python
import functools

import jax
import jax.numpy as jnp
from jax import lax
from jax.experimental import pallas as pl
from jax.experimental.pallas import tpu as pltpu
from jax.sharding import PartitionSpec as P

NORM_EPS = 1e-05
BF = jnp.bfloat16
F32 = jnp.float32
MESH_ID = pl.DeviceIdType.MESH
NZ, NU, NY = 8, 8, 4
SL = 6
SLP = 8
CH = NU * SL
ROWS = 16
EDGE = 32
HOME = 6
PACE = 3
EARLY = 4


def remote(src, dst, send, recv, ep, tp):
    return pltpu.make_async_remote_copy(
        src_ref=src,
        dst_ref=dst,
        send_sem=send,
        recv_sem=recv,
        device_id=(ep, tp),
        device_id_type=MESH_ID,
    )


ORDER = (2, 6, 5, 3, 4, 7, 1, 0)
LOCAL = ORDER.index(0)
PACKED = sum(far << (4 * k) for k, far in enumerate(ORDER))


def shift_of(k):
    return lax.shift_right_logical(jnp.int32(PACKED), jnp.int32(4) * k) & 7


def silu(a):
    return a * lax.logistic(a)


def scaled(values, gain):
    center = values - jnp.mean(values, axis=-1, keepdims=True)
    spread = jnp.mean(center * center, axis=-1, keepdims=True)
    return center * lax.rsqrt(spread + NORM_EPS) * gain


def dot(a, b):
    return jnp.dot(a, b, preferred_element_type=F32)


def body(
    conv_hbm,
    taps_hbm,
    conv_g_hbm,
    ow_hbm,
    moe_hbm,
    moe_g_hbm,
    gate_hbm,
    up_hbm,
    down_hbm,
    sgate_hbm,
    sup_hbm,
    sdown_hbm,
    index_hbm,
    weight_hbm,
    conv_out,
    moe_out,
    conv_in,
    conv_k,
    conv_g,
    moe_in,
    moe_g,
    index,
    weight,
    ow,
    gate,
    up,
    down,
    sgate,
    sup,
    sdown,
    halo,
    cpad,
    mixed,
    normed,
    own,
    select,
    xd,
    xdr,
    disp,
    xin,
    hid,
    part,
    rsa,
    rsb,
    ret,
    back,
    xs,
    xr,
    pick,
    shared,
    weights,
    conv_held,
    moe_held,
    ld,
    halo_sem,
    xd_s,
    xd_r,
    cv_s,
    cv_r,
    zd_s,
    zd_r,
    ag_s,
    ag_r,
    rs_s,
    rs_r,
    zr_s,
    zr_r,
    xr_s,
    xr_r,
    out_sem,
):
    tokens, width = moe_in.shape
    half = width // 2
    wide = 512
    every, low, high = pl.ds(0, width), pl.ds(0, half), pl.ds(half, half)
    ep = lax.axis_index("ep")
    y = lax.axis_index("tp")
    z, u = lax.div(ep, NU), lax.rem(ep, NU)
    yp, ym, yo = lax.rem(y + 1, NY), lax.rem(y + NY - 1, NY), lax.rem(y + 2, NY)

    def at_zu(zz, uu):
        return zz * NU + uu

    flat = ep * NY + y
    count = NZ * NU * NY
    ahead = lax.rem(flat + 1, count)
    behind = lax.rem(flat + count - 1, count)

    barrier = pltpu.get_barrier_semaphore()

    def greet(e, t):
        pl.semaphore_signal(barrier, inc=1, device_id=(e, t), device_id_type=MESH_ID)

    greet(ep, yp)
    greet(ep, ym)
    for d in range(1, NZ):
        greet(at_zu(lax.rem(z + d, NZ), u), y)
    for d in range(1, NU):
        greet(at_zu(z, lax.rem(u + d, NU)), y)
    greet(lax.div(ahead, NY), lax.rem(ahead, NY))
    greet(lax.div(behind, NY), lax.rem(behind, NY))

    loads = [
        pltpu.make_async_copy(source, target, ld.at[n])
        for n, (source, target) in enumerate(
            (
                (conv_hbm, conv_in),
                (taps_hbm, conv_k),
                (conv_g_hbm, conv_g),
                (index_hbm, index),
                (weight_hbm, weight),
                (moe_hbm, moe_in),
                (moe_g_hbm, moe_g),
                (gate_hbm.at[0], gate),
                (up_hbm.at[0], up),
                (down_hbm.at[0], down),
                (ow_hbm, ow),
                (sgate_hbm, sgate),
                (sup_hbm, sup),
                (sdown_hbm, sdown),
            )
        )
    ]
    for load in loads:
        load.start()

    blocks = width // 128
    taps = conv_k.shape[0]
    for load in loads[0:3]:
        load.wait()

    def fill(b, _):
        columns = pl.ds(pl.multiple_of(b * 128, 128), 128)
        cpad[b, EDGE : EDGE + tokens, :] = conv_in[:, columns].astype(F32)
        return 0

    lax.fori_loop(0, blocks, fill, 0)

    def convolve(begin, length):
        def one(b, _):
            columns = pl.ds(pl.multiple_of(b * 128, 128), 128)
            total = jnp.zeros((length, 128), F32)
            for k in range(taps):
                start = begin + EDGE + 1 - taps + k
                total = total + cpad[b, start : start + length, :] * conv_k[k : k + 1, columns]
            mixed[begin : begin + length, columns] = total
            return 0

        lax.fori_loop(0, blocks, one, 0)

        def conv_norm(r, _):
            rows = pl.ds(pl.multiple_of(begin + r * ROWS, ROWS), ROWS)
            normed[y, rows, :] = silu(scaled(mixed[rows, :], conv_g[...])).astype(BF)
            return 0

        lax.fori_loop(0, length // ROWS, conv_norm, 0, unroll=2)

    def conv_copy(n, slot, columns, to):
        rows = pl.ds(EDGE, tokens - EDGE) if n < 4 else pl.ds(0, EDGE)
        where = normed.at[slot, rows, columns]
        return remote(where, where, cv_s.at[0], cv_r.at[n], ep, to)

    conv_sends = [
        conv_copy(0, y, every, yp),
        conv_copy(1, y, every, ym),
        conv_copy(2, ym, low, yp),
        conv_copy(3, yp, high, ym),
        conv_copy(4, y, every, yp),
        conv_copy(5, y, every, ym),
        conv_copy(6, ym, low, yp),
        conv_copy(7, yp, high, ym),
    ]
    convolve(EDGE, tokens - EDGE)

    pl.semaphore_wait(barrier, NZ - 1 + NU - 1 + 4)

    halo_copy = remote(
        conv_in.at[pl.ds(tokens - EDGE, EDGE), :],
        halo,
        halo_sem.at[0],
        halo_sem.at[1],
        lax.div(ahead, NY),
        lax.rem(ahead, NY),
    )
    halo_copy.start()
    conv_sends[0].start()
    conv_sends[1].start()

    loads[3].wait()
    loads[4].wait()

    mine = index[:, pl.ds(pl.multiple_of(y * tokens, tokens), tokens)]
    expert = lax.broadcasted_iota(jnp.int32, (NZ * NU, tokens), 0)
    first = expert == mine[0:1, :]
    second = expert == mine[1:2, :]
    named = (first | second).astype(F32).astype(BF)
    row_i = lax.broadcasted_iota(jnp.int32, (tokens, tokens), 0)
    col_i = lax.broadcasted_iota(jnp.int32, (tokens, tokens), 1)
    rank = dot(named, (row_i < col_i).astype(F32).astype(BF))
    rank_first = jnp.sum(jnp.where(first, rank, 0.0), axis=0, keepdims=True)
    rank_second = jnp.sum(jnp.where(second, rank, 0.0), axis=0, keepdims=True)
    place_first = mine[0:1, :] * SLP + rank_first.astype(jnp.int32)
    place_second = mine[1:2, :] * SLP + rank_second.astype(jnp.int32)
    place = lax.broadcasted_iota(jnp.int32, (NZ * NU * SLP, tokens), 0)
    hits = ((place == place_first) | (place == place_second)).astype(F32).astype(BF)
    select[...] = hits.reshape(NZ, NU * SLP, tokens)

    share = weight[...]
    share_a = share.astype(BF).astype(F32)
    share_b = (share - share_a).astype(BF).astype(F32)
    share_c = share - share_a - share_b
    line = lax.broadcasted_iota(jnp.int32, (16, tokens), 0)
    table = jnp.zeros((16, tokens), F32)
    for n, values in enumerate(
        (
            mine[0:1, :].astype(F32),
            mine[1:2, :].astype(F32),
            rank_first,
            rank_second,
            share_a[0:1, :],
            share_a[1:2, :],
            share_b[0:1, :],
            share_b[1:2, :],
            share_c[0:1, :],
            share_c[1:2, :],
        )
    ):
        table = jnp.where(line == n, values, table)
    turned = lax.dot_general(
        (row_i == col_i).astype(F32).astype(BF),
        table.astype(BF),
        (((1,), (1,)), ((), ())),
        preferred_element_type=F32,
    )
    weights[:, 0:2] = turned[:, 4:6] + turned[:, 6:8] + turned[:, 8:10]
    places = (turned[:, 0:2] * SLP + turned[:, 2:4]).astype(jnp.int32)
    spot = lax.broadcasted_iota(jnp.int32, (tokens, NZ * NU * SLP), 1)
    pick[0:tokens, :] = (spot == places[:, 0:1]).astype(F32).astype(BF)
    pick[tokens : 2 * tokens, :] = (spot == places[:, 1:2]).astype(F32).astype(BF)

    loads[5].wait()
    loads[6].wait()

    def norm_rows(r, _):
        rows = pl.ds(pl.multiple_of(r * ROWS, ROWS), ROWS)
        own[rows, :] = scaled(moe_in[rows, :].astype(F32), moe_g[...]).astype(BF)
        return 0

    lax.fori_loop(0, tokens // ROWS, norm_rows, 0, unroll=4)

    def xd_copy(k, d):
        zz = lax.rem(z + shift_of(k), NZ)
        v = lax.rem(u + d, NU)
        return remote(
            xd.at[zz, v], xdr.at[zz, u], xd_s.at[0], xd_r.at[k], at_zu(z, v), y
        )

    def send_rows(k, _):
        zz = lax.rem(z + shift_of(k), NZ)
        for b in range(width // wide):
            columns = slice(b * wide, (b + 1) * wide)
            rows = dot(select[zz], own[:, columns])
            xd[zz, :, :, columns] = rows.reshape(NU, SLP, wide).astype(BF)

        def one(d, _):
            xd_copy(k, d).start()
            return 0

        return lax.fori_loop(1, NU, one, 0)

    lax.fori_loop(0, PACE, send_rows, 0)

    halo_copy.wait_recv()
    keep = jnp.where(flat == 0, 0.0, 1.0)

    def fill_edge(b, _):
        columns = pl.ds(pl.multiple_of(b * 128, 128), 128)
        cpad[b, 0:EDGE, :] = halo[:, columns].astype(F32) * keep
        return 0

    lax.fori_loop(0, blocks, fill_edge, 0)
    convolve(0, EDGE)
    conv_sends[4].start()
    conv_sends[5].start()

    wide_r = lax.broadcasted_iota(jnp.int32, (NU * SLP, CH), 0)
    wide_c = lax.broadcasted_iota(jnp.int32, (NU * SLP, CH), 1)
    spread = ((wide_r & 7) < SL) & (wide_c == (wide_r >> 3) * SL + (wide_r & 7))
    spread = spread.astype(F32).astype(BF)
    pack_r = lax.broadcasted_iota(jnp.int32, (CH, NU * SLP), 0)
    pack_c = lax.broadcasted_iota(jnp.int32, (CH, NU * SLP), 1)
    pack = ((pack_c & 7) < SL) & (pack_r == (pack_c >> 3) * SL + (pack_c & 7))
    pack = pack.astype(F32).astype(BF)

    def disp_copy(k):
        target = lax.rem(z + shift_of(k), NZ)
        return remote(
            disp.at[k], xin.at[k, y], zd_s.at[0], zd_r.at[k], at_zu(target, u), y
        )

    def rows_along(k):
        zz = lax.rem(z + shift_of(k), NZ)

        @pl.when(k < NZ - PACE)
        def _():
            send_rows(k + PACE, 0)

        landed = xdr.at[zz, pl.ds(0, NU - 1)]
        remote(landed, landed, xd_s.at[0], xd_r.at[k], ep, yp).wait_recv()
        xdr[zz, u] = xd[zz, u]

        def narrow(b, _):
            columns = pl.ds(pl.multiple_of(b * wide, wide), wide)
            rows = xdr[zz, :, :, columns].astype(F32).reshape(NU * SLP, wide).astype(BF)
            disp[k, :, columns] = dot(pack, rows).astype(BF)
            return 0

        lax.fori_loop(0, width // wide, narrow, 0, unroll=True)

        @pl.when(k != LOCAL)
        def _():
            disp_copy(k).start()

        @pl.when(k == LOCAL)
        def _():
            xin[k, y] = disp[k]

    def ag_copy(k, n, slot, columns, to):
        where = xin.at[k, slot, :, columns]
        return remote(where, where, ag_s.at[0], ag_r.at[k, n], ep, to)

    def ag_sends(k):
        return [
            ag_copy(k, 0, y, every, yp),
            ag_copy(k, 1, y, every, ym),
            ag_copy(k, 2, ym, low, yp),
            ag_copy(k, 3, yp, high, ym),
        ]

    def rows_out(k):
        @pl.when(k != LOCAL)
        def _():
            disp_copy(k).wait_recv()

        sends = ag_sends(k)
        sends[0].start()
        sends[1].start()

    rows_along(jnp.int32(0))
    rows_along(jnp.int32(1))
    rows_along(jnp.int32(2))
    conv_copy(0, ym, every, yp).wait_recv()
    conv_sends[2].start()
    conv_copy(1, yp, every, ym).wait_recv()
    conv_sends[3].start()
    rows_along(jnp.int32(3))
    rows_out(jnp.int32(0))
    conv_copy(4, ym, every, yp).wait_recv()
    conv_sends[6].start()
    conv_copy(5, yp, every, ym).wait_recv()
    conv_sends[7].start()
    rows_out(jnp.int32(1))
    for load in loads[7:]:
        load.wait()

    def rs_sends(k):
        return [
            remote(part.at[k, yo, :, low], rsa.at[k, 0], rs_s.at[0], rs_r.at[k, 0], ep, yp),
            remote(part.at[k, yo, :, high], rsa.at[k, 1], rs_s.at[0], rs_r.at[k, 1], ep, ym),
            remote(part.at[k, yp], rsb.at[k, 0], rs_s.at[0], rs_r.at[k, 2], ep, yp),
            remote(part.at[k, ym], rsb.at[k, 1], rs_s.at[0], rs_r.at[k, 3], ep, ym),
        ]

    def ret_copy(k, h):
        source = lax.rem(z - shift_of(k) + NZ, NZ)
        columns = (low, high)[h]
        return remote(
            ret.at[k, :, columns],
            back.at[k, :, columns],
            zr_s.at[0],
            zr_r.at[k, h],
            at_zu(source, u),
            y,
        )

    def xr_copy(k, d, columns):
        zz = lax.rem(z + shift_of(k), NZ)
        v = lax.rem(u + d, NU)
        return remote(
            xs.at[k, v, :, columns],
            xr.at[zz, u, :, columns],
            xr_s.at[0],
            xr_r.at[k],
            at_zu(z, v),
            y,
        )

    def rows_on(k):
        sends = ag_sends(k)
        ag_copy(k, 0, ym, every, yp).wait_recv()
        sends[2].start()
        ag_copy(k, 1, yp, every, ym).wait_recv()
        sends[3].start()

    def experts(k):
        ag_copy(k, 2, yo, low, yp).wait_recv()
        ag_copy(k, 3, yo, high, ym).wait_recv()
        rows = xin[k].reshape(NY * CH, width)
        ff = gate.shape[1]
        for b in range(ff // 256):
            columns = slice(b * 256, (b + 1) * 256)
            hid[:, columns] = (silu(dot(rows, gate[:, columns])) * dot(rows, up[:, columns])).astype(BF)

        def project(b, _):
            columns = pl.ds(pl.multiple_of(b * wide, wide), wide)
            out = dot(hid[...], down[:, columns]).astype(BF)
            part[k, :, :, columns] = out.reshape(NY, CH, wide)
            return 0

        lax.fori_loop(0, width // wide, project, 0)
        sends = rs_sends(k)
        sends[0].start()
        sends[1].start()

    def parts_on(k):
        sends = rs_sends(k)
        sends[0].wait_recv()
        kept = part[k, yp, :, low].astype(F32) + rsa[k, 0].astype(F32)
        part[k, yp, :, low] = kept.astype(BF)
        sends[2].start()
        sends[1].wait_recv()
        kept = part[k, ym, :, high].astype(F32) + rsa[k, 1].astype(F32)
        part[k, ym, :, high] = kept.astype(BF)
        sends[3].start()

    def results(k):
        sends = rs_sends(k)
        sends[2].wait_recv()
        sends[3].wait_recv()
        for h, columns in enumerate((low, high)):
            total = part[k, y, :, columns].astype(F32) + rsb[k, 0, :, columns].astype(F32)
            total = (total + rsb[k, 1, :, columns].astype(F32)).astype(BF)

            @pl.when(k != LOCAL)
            def _():
                ret[k, :, columns] = total
                ret_copy(k, h).start()

            @pl.when(k == LOCAL)
            def _():
                back[k, :, columns] = total

    def results_home(k):
        for h, columns in enumerate((low, high)):

            @pl.when(k != LOCAL)
            def _():
                ret_copy(k, h).wait_recv()

            for b in range(half // wide):
                some = pl.ds(h * half + b * wide, wide)
                out = dot(spread, back[k, :, some])
                xs[k, :, :, some] = out.reshape(NU, SLP, wide).astype(BF)

            def send(d, _):
                xr_copy(k, d, columns).start()
                return 0

            lax.fori_loop(1, NU, send, 0)
        xr[lax.rem(z + shift_of(k), NZ), u] = xs[k, u]

    conv_save = pltpu.make_async_copy(conv_held, conv_out, out_sem.at[0])

    def moe_save(b):
        columns = pl.ds(pl.multiple_of(b * wide, wide), wide)
        return pltpu.make_async_copy(moe_held.at[b], moe_out.at[:, columns], out_sem.at[b + 1])

    def beside():
        rows = own[...]
        hidden = (silu(dot(rows, sgate[...])) * dot(rows, sup[...])).astype(BF)
        shared[...] = dot(hidden, sdown[...])
        conv_copy(2, yo, low, yp).wait_recv()
        conv_copy(3, yo, high, ym).wait_recv()
        conv_copy(6, yo, low, yp).wait_recv()
        conv_copy(7, yo, high, ym).wait_recv()

        def project(b, _):
            rows = pl.ds(pl.multiple_of(b * tokens, tokens), tokens)
            conv_held[rows, :] = dot(normed[b], ow[...]).astype(BF)
            return 0

        lax.fori_loop(0, NY, project, 0)
        conv_save.start()

    def stage(i, lag, act):
        k = i - lag

        @pl.when((k >= 0) & (k < NZ))
        def _():
            act(k)

    def step(i, _):
        stage(i, 1, rows_on)

        @pl.when((i >= 2) & (i < NZ))
        def _():
            rows_out(i)

        stage(i, 2, experts)
        stage(i, 3, parts_on)
        stage(i, -EARLY, rows_along)

        @pl.when(i == LOCAL + 4)
        def _():
            results_home(i - HOME)

        stage(i, 4, results)

        @pl.when(i == LOCAL + 4)
        def _():
            results_home(i - 4)

        @pl.when((i >= HOME) & (i != LOCAL + 4))
        def _():
            results_home(i - HOME)

        @pl.when(i == 4)
        def _():
            beside()

        return 0

    lax.fori_loop(0, NZ - 1 + HOME, step, 0)

    def arrived(k, _):
        landed = xr.at[lax.rem(z + shift_of(k), NZ), pl.ds(0, NU - 1)]
        remote(landed, landed, xr_s.at[0], xr_r.at[k], ep, yp).wait_recv()
        return 0

    lax.fori_loop(0, NZ, arrived, 0)

    def combine(b, _):
        columns = pl.ds(pl.multiple_of(b * wide, wide), wide)
        rows = xr[:, :, :, columns].astype(F32).reshape(NZ * NU * SLP, wide).astype(BF)
        both = dot(pick[...], rows)
        routed = both[0:tokens] * weights[:, 0:1] + both[tokens : 2 * tokens] * weights[:, 1:2]
        moe_held[b] = (shared[:, columns] + routed).astype(BF)
        moe_save(b).start()
        return 0

    lax.fori_loop(0, width // wide, combine, 0, unroll=2)

    halo_copy.wait_send()
    sent = pl.ds(0, NU - 1)
    for left, semaphore in (
        (normed.at[pl.ds(0, 3)], cv_s),
        (xd.at[sent], xd_s),
        (disp.at[sent], zd_s),
        (xin.at[:, pl.ds(0, 3)], ag_s),
        (part.at[:, pl.ds(0, 3)], rs_s),
        (ret.at[sent], zr_s),
        (xs.at[sent], xr_s),
    ):
        remote(left, left, semaphore.at[0], halo_sem.at[1], ep, yp).wait_send()
    conv_save.wait()
    for b in range(width // wide):
        moe_save(b).wait()


def hand_on(conv_from, moe_from, conv_to, moe_to, conv_held, moe_held, semaphores):
    copies = [
        pltpu.make_async_copy(source, target, semaphores.at[n])
        for n, (source, target) in enumerate(
            (
                (conv_from, conv_held),
                (moe_from, moe_held),
                (conv_held, conv_to),
                (moe_held, moe_to),
            )
        )
    ]
    copies[0].start()
    copies[1].start()
    copies[0].wait()
    copies[2].start()
    copies[1].wait()
    copies[3].start()
    copies[2].wait()
    copies[3].wait()


def on_device(*args):
    (
        conv_input,
        conv_kernel,
        conv_gain,
        out_weight,
        moe_input,
        moe_gain,
        expert_gate,
        expert_up,
        expert_down,
        shared_gate,
        shared_up,
        shared_down,
        expert_index,
        routing_weight,
    ) = args
    tokens, width = moe_input.shape
    half = width // 2
    ff = expert_gate.shape[2]
    cols = out_weight.shape[1]
    vm = lambda *shape, dtype=BF: pltpu.VMEM(shape, dtype)
    dma = lambda *shape: pltpu.SemaphoreType.DMA(shape)
    in_hbm = pl.BlockSpec(memory_space=pl.ANY)
    operands = (
        (conv_input, in_hbm),
        (conv_kernel, in_hbm),
        (conv_gain.reshape(1, width), in_hbm),
        (out_weight, in_hbm),
        (moe_input, in_hbm),
        (moe_gain.reshape(1, width), in_hbm),
        (expert_gate, in_hbm),
        (expert_up, in_hbm),
        (expert_down, in_hbm),
        (shared_gate, in_hbm),
        (shared_up, in_hbm),
        (shared_down, in_hbm),
        (expert_index.T, in_hbm),
        (routing_weight.T, in_hbm),
    )
    scratch = [
        vm(tokens, width),
        vm(*conv_kernel.shape, dtype=F32),
        vm(1, width, dtype=F32),
        vm(tokens, width),
        vm(1, width, dtype=F32),
        vm(*expert_index.shape[::-1], dtype=jnp.int32),
        vm(*routing_weight.shape[::-1], dtype=F32),
        vm(width, cols),
        vm(width, ff),
        vm(width, ff),
        vm(ff, width),
        vm(*shared_gate.shape),
        vm(*shared_up.shape),
        vm(*shared_down.shape),
        vm(EDGE, width),
        vm(width // 128, EDGE + tokens, 128, dtype=F32),
        vm(tokens, width, dtype=F32),
        vm(NY, tokens, width),
        vm(tokens, width),
        vm(NZ, NU * SLP, tokens),
        vm(NZ, NU, SLP, width),
        vm(NZ, NU, SLP, width),
        vm(NZ, CH, width),
        vm(NZ, NY, CH, width),
        vm(NY * CH, ff),
        vm(NZ, NY, CH, width),
        vm(NZ, 2, CH, half),
        vm(NZ, 2, CH, width),
        vm(NZ, CH, width),
        vm(NZ, CH, width),
        vm(NZ, NU, SLP, width),
        vm(NZ, NU, SLP, width),
        vm(2 * tokens, NZ * NU * SLP),
        vm(tokens, width, dtype=F32),
        vm(tokens, 128, dtype=F32),
        vm(NY * tokens, cols),
        vm(width // 512, tokens, 512),
        dma(14),
        dma(2),
        dma(1),
        dma(NZ),
        dma(1),
        dma(8),
        dma(1),
        dma(NZ),
        dma(1),
        dma(NZ, 4),
        dma(1),
        dma(NZ, 4),
        dma(1),
        dma(NZ, 2),
        dma(1),
        dma(NZ),
        dma(1 + width // 512),
    ]
    shapes = (
        jax.ShapeDtypeStruct((NY * tokens, cols), BF),
        jax.ShapeDtypeStruct((tokens, width), BF),
    )
    results = pl.pallas_call(
        body,
        out_shape=shapes,
        in_specs=[spec for _, spec in operands],
        out_specs=(in_hbm, in_hbm),
        scratch_shapes=scratch,
        compiler_params=pltpu.CompilerParams(
            collective_id=0, has_side_effects=True, vmem_limit_bytes=67043328
        ),
    )(*[array for array, _ in operands])
    return pl.pallas_call(
        hand_on,
        out_shape=shapes,
        in_specs=[in_hbm, in_hbm],
        out_specs=(in_hbm, in_hbm),
        scratch_shapes=[vm(*shape.shape) for shape in shapes] + [dma(4)],
    )(*results)


def solution(mesh):
    in_specs = (
        P(("ep", "tp"), None),
        P(),
        P(),
        P(None, "tp"),
        P(("ep", "tp"), None),
        P(),
        P("ep", None, "tp"),
        P("ep", None, "tp"),
        P("ep", "tp", None),
        P(),
        P(),
        P(),
        P("ep", None),
        P(("ep", "tp"), None),
    )
    out_specs = (P("ep", "tp"), P(("ep", "tp"), None))
    return jax.shard_map(
        on_device, mesh=mesh, in_specs=in_specs, out_specs=out_specs, check_vma=False
    )
```

time: 163 us -> 155 us (0.951)
  the two profiles are of different devices: /device:TPU:1 before, /device:TPU:165 now
where the time goes in v3:
time: 155 us
  Pallas kernels  154 us (99%)
    pallas_call x1, Pallas kernels, on_device(): pl.pallas_call(body, out_shape=shapes, in_specs=[spec for _, spec in oper...  152 us

profile of v3, /device:TPU:165, one launch (start us, length us, event | category | flops | bytes accessed | tf_op | source)
XLA Modules:
  0.0 154.9 jit_solution(11678874640124794368)
XLA Ops:
  0.6 152.3 %shard_map.149 = (bf16[512,512]{1,0:T(8,128)(2,1)}, bf16[128,2048]{1,0:T(8,128)(2,1)}) custom-call(bf16[128,2048]{1,0:T(8,128)(2,1)} %conv_hbm.1, f32[31,2048]{1,0:T(8,128)} %taps_hbm.1, f32[1,2048]{1,0:T(1,128)} %bitcast.4, bf16[2048,512]{1,0:T(8,128)(2,1)} %ow_hbm.1, bf16[128,2048]{1,0:T(8,128)(2,1)} %moe_hbm.1, f32[1,2048]{1,0:T(1,128)} %bitcast.5, ...), custom_call_target="tpu_custom_call" | custom-call | tf_op jit(solution)/shard_map/pallas_call | solution.py:751
  152.9 2.0 %shard_map.150 = (bf16[512,512]{1,0:T(8,128)(2,1)}, bf16[128,2048]{1,0:T(8,128)(2,1)}) custom-call(bf16[512,512]{1,0:T(8,128)(2,1)} %get-tuple-element.4.conv_from, bf16[128,2048]{1,0:T(8,128)(2,1)} %get-tuple-element.5.moe_from), custom_call_target="tpu_custom_call" | custom-call | tf_op jit(solution)/shard_map/pallas_call | solution.py:761

commit v4 on v3

--- a/solution.py
+++ b/solution.py
@@ -33,7 +33,7 @@
     )
 
 
-ORDER = (2, 6, 5, 3, 4, 7, 1, 0)
+ORDER = (0, 6, 3, 5, 4, 2, 7, 1)
 LOCAL = ORDER.index(0)
 PACKED = sum(far << (4 * k) for k, far in enumerate(ORDER))
 
@@ -406,19 +406,9 @@
         sends[1].start()
 
     rows_along(jnp.int32(0))
-    rows_along(jnp.int32(1))
-    rows_along(jnp.int32(2))
-    conv_copy(0, ym, every, yp).wait_recv()
-    conv_sends[2].start()
-    conv_copy(1, yp, every, ym).wait_recv()
-    conv_sends[3].start()
-    rows_along(jnp.int32(3))
     rows_out(jnp.int32(0))
-    conv_copy(4, ym, every, yp).wait_recv()
-    conv_sends[6].start()
-    conv_copy(5, yp, every, ym).wait_recv()
-    conv_sends[7].start()
-    rows_out(jnp.int32(1))
+    for k in range(1, EARLY):
+        rows_along(jnp.int32(k))
     for load in loads[7:]:
         load.wait()
 
@@ -538,17 +528,29 @@
         rows = own[...]
         hidden = (silu(dot(rows, sgate[...])) * dot(rows, sup[...])).astype(BF)
         shared[...] = dot(hidden, sdown[...])
-        conv_copy(2, yo, low, yp).wait_recv()
-        conv_copy(3, yo, high, ym).wait_recv()
-        conv_copy(6, yo, low, yp).wait_recv()
-        conv_copy(7, yo, high, ym).wait_recv()
-
-        def project(b, _):
-            rows = pl.ds(pl.multiple_of(b * tokens, tokens), tokens)
-            conv_held[rows, :] = dot(normed[b], ow[...]).astype(BF)
+        for n, slot in enumerate((ym, yp)):
+            conv_copy(n, slot, every, yp).wait_recv()
+            conv_copy(n + 4, slot, every, yp).wait_recv()
+
+        def project(n, _):
+            conv_project(lax.rem(y + NY - 1 + n, NY))
             return 0
 
-        lax.fori_loop(0, NY, project, 0)
+        lax.fori_loop(0, 3, project, 0)
+
+    def conv_project(b):
+        rows = pl.ds(pl.multiple_of(b * tokens, tokens), tokens)
+        conv_held[rows, :] = dot(normed[b], ow[...]).astype(BF)
+
+    def conv_forward():
+        for n in (2, 3, 6, 7):
+            conv_sends[n].start()
+
+    def conv_last():
+        for n in (2, 6):
+            conv_copy(n, yo, low, yp).wait_recv()
+            conv_copy(n + 1, yo, high, ym).wait_recv()
+        conv_project(yo)
         conv_save.start()
 
     def stage(i, lag, act):
@@ -561,27 +563,20 @@
     def step(i, _):
         stage(i, 1, rows_on)
 
-        @pl.when((i >= 2) & (i < NZ))
+        @pl.when((i >= 1) & (i < NZ))
         def _():
             rows_out(i)
 
         stage(i, 2, experts)
         stage(i, 3, parts_on)
+
+        @pl.when(i == NZ + 2)
+        def _():
+            conv_forward()
+
         stage(i, -EARLY, rows_along)
-
-        @pl.when(i == LOCAL + 4)
-        def _():
-            results_home(i - HOME)
-
         stage(i, 4, results)
-
-        @pl.when(i == LOCAL + 4)
-        def _():
-            results_home(i - 4)
-
-        @pl.when((i >= HOME) & (i != LOCAL + 4))
-        def _():
-            results_home(i - HOME)
+        stage(i, HOME, results_home)
 
         @pl.when(i == 4)
         def _():
@@ -589,7 +584,8 @@
 
         return 0
 
-    lax.fori_loop(0, NZ - 1 + HOME, step, 0)
+    lax.fori_loop(0, NZ + HOME, step, 0)
+    conv_last()
 
     def arrived(k, _):
         landed = xr.at[lax.rem(z + shift_of(k), NZ), pl.ds(0, NU - 1)]

time: 155 us -> 150 us (0.968)
  the two profiles are of different devices: /device:TPU:165 before, /device:TPU:1 now
where the time goes in v4:
time: 150 us
  Pallas kernels  149 us (99%)
    pallas_call x1, Pallas kernels, on_device(): pl.pallas_call(body, out_shape=shapes, in_specs=[spec for _, spec in oper...  147 us

profile of v4, /device:TPU:1, one launch (start us, length us, event | category | flops | bytes accessed | tf_op | source)
XLA Modules:
  0.0 149.5 jit_solution(5307936598726692698)
XLA Ops:
  0.6 146.8 %shard_map.149 = (bf16[512,512]{1,0:T(8,128)(2,1)}, bf16[128,2048]{1,0:T(8,128)(2,1)}) custom-call(bf16[128,2048]{1,0:T(8,128)(2,1)} %conv_hbm.1, f32[31,2048]{1,0:T(8,128)} %taps_hbm.1, f32[1,2048]{1,0:T(1,128)} %bitcast.4, bf16[2048,512]{1,0:T(8,128)(2,1)} %ow_hbm.1, bf16[128,2048]{1,0:T(8,128)(2,1)} %moe_hbm.1, f32[1,2048]{1,0:T(1,128)} %bitcast.5, ...), custom_call_target="tpu_custom_call" | custom-call | tf_op jit(solution)/shard_map/pallas_call | solution.py:747
  147.5 2.0 %shard_map.150 = (bf16[512,512]{1,0:T(8,128)(2,1)}, bf16[128,2048]{1,0:T(8,128)(2,1)}) custom-call(bf16[512,512]{1,0:T(8,128)(2,1)} %get-tuple-element.4.conv_from, bf16[128,2048]{1,0:T(8,128)(2,1)} %get-tuple-element.5.moe_from), custom_call_target="tpu_custom_call" | custom-call | tf_op jit(solution)/shard_map/pallas_call | solution.py:757

commit v5 on v4

--- a/solution.py
+++ b/solution.py
@@ -108,8 +108,6 @@
     pick,
     shared,
     weights,
-    conv_held,
-    moe_held,
     ld,
     halo_sem,
     xd_s,
@@ -126,7 +124,6 @@
     zr_r,
     xr_s,
     xr_r,
-    out_sem,
 ):
     tokens, width = moe_in.shape
     half = width // 2
@@ -327,7 +324,9 @@
 
         return lax.fori_loop(1, NU, one, 0)
 
-    lax.fori_loop(0, PACE, send_rows, 0)
+    send_rows(jnp.int32(1), 0)
+    send_rows(jnp.int32(0), 0)
+    send_rows(jnp.int32(2), 0)
 
     halo_copy.wait_recv()
     keep = jnp.where(flat == 0, 0.0, 1.0)
@@ -357,12 +356,12 @@
             disp.at[k], xin.at[k, y], zd_s.at[0], zd_r.at[k], at_zu(target, u), y
         )
 
-    def rows_along(k):
+    def rows_along(k, later):
         zz = lax.rem(z + shift_of(k), NZ)
 
-        @pl.when(k < NZ - PACE)
+        @pl.when(later < NZ)
         def _():
-            send_rows(k + PACE, 0)
+            send_rows(later, 0)
 
         landed = xdr.at[zz, pl.ds(0, NU - 1)]
         remote(landed, landed, xd_s.at[0], xd_r.at[k], ep, yp).wait_recv()
@@ -405,10 +404,11 @@
         sends[0].start()
         sends[1].start()
 
-    rows_along(jnp.int32(0))
+    rows_along(jnp.int32(1), jnp.int32(3))
+    rows_along(jnp.int32(0), jnp.int32(4))
     rows_out(jnp.int32(0))
-    for k in range(1, EARLY):
-        rows_along(jnp.int32(k))
+    rows_along(jnp.int32(2), jnp.int32(5))
+    rows_along(jnp.int32(3), jnp.int32(6))
     for load in loads[7:]:
         load.wait()
 
@@ -518,12 +518,6 @@
             lax.fori_loop(1, NU, send, 0)
         xr[lax.rem(z + shift_of(k), NZ), u] = xs[k, u]
 
-    conv_save = pltpu.make_async_copy(conv_held, conv_out, out_sem.at[0])
-
-    def moe_save(b):
-        columns = pl.ds(pl.multiple_of(b * wide, wide), wide)
-        return pltpu.make_async_copy(moe_held.at[b], moe_out.at[:, columns], out_sem.at[b + 1])
-
     def beside():
         rows = own[...]
         hidden = (silu(dot(rows, sgate[...])) * dot(rows, sup[...])).astype(BF)
@@ -540,7 +534,7 @@
 
     def conv_project(b):
         rows = pl.ds(pl.multiple_of(b * tokens, tokens), tokens)
-        conv_held[rows, :] = dot(normed[b], ow[...]).astype(BF)
+        conv_out[rows, :] = dot(normed[b], ow[...]).astype(BF)
 
     def conv_forward():
         for n in (2, 3, 6, 7):
@@ -551,7 +545,6 @@
             conv_copy(n, yo, low, yp).wait_recv()
             conv_copy(n + 1, yo, high, ym).wait_recv()
         conv_project(yo)
-        conv_save.start()
 
     def stage(i, lag, act):
         k = i - lag
@@ -561,12 +554,12 @@
             act(k)
 
     def step(i, _):
-        stage(i, 1, rows_on)
-
         @pl.when((i >= 1) & (i < NZ))
         def _():
             rows_out(i)
 
+        stage(i, 1, rows_on)
+
         stage(i, 2, experts)
         stage(i, 3, parts_on)
 
@@ -574,7 +567,7 @@
         def _():
             conv_forward()
 
-        stage(i, -EARLY, rows_along)
+        stage(i, -EARLY, lambda k: rows_along(k, k + PACE))
         stage(i, 4, results)
         stage(i, HOME, results_home)
 
@@ -599,8 +592,7 @@
         rows = xr[:, :, :, columns].astype(F32).reshape(NZ * NU * SLP, wide).astype(BF)
         both = dot(pick[...], rows)
         routed = both[0:tokens] * weights[:, 0:1] + both[tokens : 2 * tokens] * weights[:, 1:2]
-        moe_held[b] = (shared[:, columns] + routed).astype(BF)
-        moe_save(b).start()
+        moe_out[:, columns] = (shared[:, columns] + routed).astype(BF)
         return 0
 
     lax.fori_loop(0, width // wide, combine, 0, unroll=2)
@@ -617,31 +609,6 @@
         (xs.at[sent], xr_s),
     ):
         remote(left, left, semaphore.at[0], halo_sem.at[1], ep, yp).wait_send()
-    conv_save.wait()
-    for b in range(width // wide):
-        moe_save(b).wait()
-
-
-def hand_on(conv_from, moe_from, conv_to, moe_to, conv_held, moe_held, semaphores):
-    copies = [
-        pltpu.make_async_copy(source, target, semaphores.at[n])
-        for n, (source, target) in enumerate(
-            (
-                (conv_from, conv_held),
-                (moe_from, moe_held),
-                (conv_held, conv_to),
-                (moe_held, moe_to),
-            )
-        )
-    ]
-    copies[0].start()
-    copies[1].start()
-    copies[0].wait()
-    copies[2].start()
-    copies[1].wait()
-    copies[3].start()
-    copies[2].wait()
-    copies[3].wait()
 
 
 def on_device(*args):
@@ -720,8 +687,6 @@
         vm(2 * tokens, NZ * NU * SLP),
         vm(tokens, width, dtype=F32),
         vm(tokens, 128, dtype=F32),
-        vm(NY * tokens, cols),
-        vm(width // 512, tokens, 512),
         dma(14),
         dma(2),
         dma(1),
@@ -738,30 +703,22 @@
         dma(NZ, 2),
         dma(1),
         dma(NZ),
-        dma(1 + width // 512),
     ]
     shapes = (
         jax.ShapeDtypeStruct((NY * tokens, cols), BF),
         jax.ShapeDtypeStruct((tokens, width), BF),
     )
-    results = pl.pallas_call(
+    in_vmem = pl.BlockSpec(memory_space=pltpu.VMEM)
+    return pl.pallas_call(
         body,
-        out_shape=shapes,
+        out_shape=tuple(pltpu.VMEM(shape.shape, BF) for shape in shapes),
         in_specs=[spec for _, spec in operands],
-        out_specs=(in_hbm, in_hbm),
+        out_specs=(in_vmem, in_vmem),
         scratch_shapes=scratch,
         compiler_params=pltpu.CompilerParams(
-            collective_id=0, has_side_effects=True, vmem_limit_bytes=67043328
+            collective_id=0, has_side_effects=True, vmem_limit_bytes=56 * 2**20
         ),
     )(*[array for array, _ in operands])
-    return pl.pallas_call(
-        hand_on,
-        out_shape=shapes,
-        in_specs=[in_hbm, in_hbm],
-        out_specs=(in_hbm, in_hbm),
-        scratch_shapes=[vm(*shape.shape) for shape in shapes] + [dma(4)],
-    )(*results)
-
 
 def solution(mesh):
     in_specs = (

time: 150 us -> 150 us (level)
  Pallas kernels: 149 us -> 147 us
  local copies, waits for them, and re-layouts: 0 us -> 1.59 us
    pallas_call x2 -> x1, Pallas kernels: 149 us -> 147 us  [on_device(): pl.pallas_call(body, out_shape=tuple((pltpu.VMEM(shape.shape, BF) for sha...]
    unnamed x0 -> x2, local copies, waits for them, and re-layouts: none -> 1.59 us
where the time goes in v5:
time: 150 us; the launch traced here: 149 us
  Pallas kernels  147 us (98%)
  local copies, waits for them, and re-layouts  1.59 us (1%)
    pallas_call x1, Pallas kernels, on_device(): pl.pallas_call(body, out_shape=tuple((pltpu.VMEM(shape.shape, BF) for sha...  147 us

profile of v5, /device:TPU:1, one launch (start us, length us, event | category | flops | bytes accessed | tf_op | source)
XLA Modules:
  0.0 149.5 jit_solution(4836420532680289842)
XLA Ops:
  0.6 147.3 %shard_map.149 = (bf16[512,512]{1,0:T(8,128)(2,1)S(1)}, bf16[128,2048]{1,0:T(8,128)(2,1)S(1)}) custom-call(bf16[128,2048]{1,0:T(8,128)(2,1)} %conv_hbm.1, f32[31,2048]{1,0:T(8,128)} %taps_hbm.1, f32[1,2048]{1,0:T(1,128)} %bitcast.4, bf16[2048,512]{1,0:T(8,128)(2,1)} %ow_hbm.1, bf16[128,2048]{1,0:T(8,128)(2,1)} %moe_hbm.1, f32[1,2048]{1,0:T(1,128)} %bitcast.5, ...), custom_call_target="tpu_custom_call" | custom-call | tf_op jit(solution)/shard_map/pallas_call | solution.py:712
  147.9 0.8 copy.18
  148.7 0.8 copy.19
